TPU v7x, 128 devices: a whole 4x4x4 slice. The times are simulated.
128 devices in a mesh: sp: 16 (over z, x), tp: 8 (over y, core).
Axes of the slice: x: 4, y: 4, z: 4, core: 2. Of those that a mesh axis runs over, the one named last changes fastest.
Arguments:
- query_small: bfloat16 [12288, 1024], P('sp', 'tp'), may hold values from -6 to 6
- key_small: bfloat16 [12288, 1024], P('sp', 'tp'), may hold values from -6 to 6
- value_small: bfloat16 [12288, 1024], P('sp', 'tp'), may hold values from -6 to 6
- gates_small: float32 [12288, 16], P('sp', 'tp'), as said below
- query_large: bfloat16 [12288, 1024], P('sp', 'tp'), may hold values from -6 to 6
- key_large: bfloat16 [12288, 1024], P('sp', 'tp'), may hold values from -6 to 6
- value_large: bfloat16 [12288, 1024], P('sp', 'tp'), may hold values from -6 to 6
- gates_large: float32 [12288, 8], P('sp', 'tp'), as said below
- residual: bfloat16 [12288, 2048], P(('sp', 'tp')), may hold values from -6 to 6
- mixer_small: bfloat16 [1024, 2048], P('tp'), may hold values from -1 to 1
- mixer_large: bfloat16 [1024, 2048], P('tp'), may hold values from -1 to 1
- mix_gain: float32 [2048], replicated, may hold values from 0.1 to 1.9
- value_weight: bfloat16 [2048, 5632], P('sp', 'tp'), may hold values from -0.125 to 0.125
- gate_weight: bfloat16 [2048, 5632], P('sp', 'tp'), may hold values from -0.125 to 0.125
- value_taps: float32 [3, 5632], P(None, 'tp'), may hold values from -3 to 3
- gate_taps: float32 [3, 5632], P(None, 'tp'), may hold values from -3 to 3
- down_weight: bfloat16 [5632, 2048], P('tp', 'sp'), may hold values from -0.078125 to 0.078125
- final_gain: float32 [2048], replicated, may hold values from 0.1 to 1.9
Outputs:
- layer_out: bfloat16 [12288, 2048], P(('sp', 'tp'))
Inputs may be any that keep to these rules, and one draw needn't show every extreme that they name: `gates_small`: each column never rises from one position to the next, and its first entry is negative. `gates_large`: each column never rises from one position to the next, and its first entry is negative.
All inputs are finite; a program needn't handle non-finite values.
Results may differ from a plain program's by a relative error of at most 0.018.
Values may be sent and summed in bfloat16 or wider, within the bound.
A program may use at most 128 MiB of HBM per device.

v0:
```python
import math

import jax
import jax.numpy as jnp
from jax import lax
from jax.sharding import Mesh
from jax.sharding import PartitionSpec as P

DS = 64
DL = 128
TP = ("tp_0", "tp_1")
SP_TP = ("sp", "tp_0", "tp_1")


residual_scale = 2.0**0.5
epsilon = 1e-05


def gather_turned(arrays, axis, dims):
    turned = [jnp.moveaxis(a, dim, 0) for a, dim in zip(arrays, dims)]
    widths = [t[0].size for t in turned]
    both = jnp.concatenate([t.reshape(-1, w) for t, w in zip(turned, widths)], axis=1)
    out = lax.all_gather(both, axis, axis=0, tiled=True)
    pieces = jnp.split(out, [sum(widths[:k]) for k in range(1, len(widths))], axis=1)
    return tuple(
        (
            jnp.moveaxis(b.reshape(-1, *t.shape[1:]), 0, dim)
            for b, t, dim in zip(pieces, turned, dims)
        )
    )


def sent_together(arrays, axis, dim, along):
    both = jnp.concatenate(arrays, axis=along)
    out, at, finished = (lax.all_gather(both, axis, axis=dim, tiled=True), 0, [])
    for a in arrays:
        finished.append(lax.slice_in_dim(out, at, at + a.shape[along], axis=along))
        at += a.shape[along]
    return tuple(finished)


def split_up(array, dim, devices):
    shape = array.shape
    pieces = array.reshape(*shape[:dim], devices, shape[dim] // devices, *shape[dim + 1 :])
    return jnp.moveaxis(pieces, dim, 0)


def laid_out(pieces, dim):
    shape = list(pieces.shape[1:])
    shape[dim] *= pieces.shape[0]
    return jnp.moveaxis(pieces, 0, dim).reshape(shape)


def moved_by_axis(pieces, axes, turns):
    shape = [lax.axis_size(a) for a in axes]
    pieces = pieces.reshape(*shape, *pieces.shape[1:])
    for k in turns:
        pieces = lax.all_to_all(pieces, axes[k], split_axis=k, concat_axis=k, tiled=True)
    return pieces.reshape(-1, *pieces.shape[len(axes) :])


def stepwise_exchange(array, axes, turns, split_dim, concat_dim):
    pieces = split_up(array, split_dim, lax.axis_size(axes))
    return laid_out(moved_by_axis(pieces, axes, turns), concat_dim)


def passed_along(value, axis, steps):
    count = lax.axis_size(axis)
    first, last = (max(0, -steps), min(count, count - steps))
    return lax.ppermute(value, axis, [(source, source + steps) for source in range(first, last)])


def norm_rows(values, gain):
    center = jnp.mean(values, axis=-1, keepdims=True)
    spread = jnp.mean(jnp.square(values - center), axis=-1, keepdims=True)
    return (values - center) * lax.rsqrt(spread + epsilon) * gain


def attend_block(
    running,
    queries,
    query_gates,
    key_rows,
    value_rows,
    key_gates,
    token_positions,
    key_first,
    head_dim,
):
    running_peak, weight_sum, weighted = running
    heads_here = query_gates.shape[1]
    span_rows = key_rows.shape[0]
    query_heads = queries.reshape(queries.shape[0], heads_here, head_dim)
    key_heads = key_rows.reshape(span_rows, heads_here, head_dim)
    value_heads = value_rows.reshape(span_rows, heads_here, head_dim)
    scores = jnp.einsum(
        "qhd,khd->hqk", query_heads, key_heads, preferred_element_type=jnp.float32
    ) * head_dim ** (-0.5)
    scores = scores + query_gates.T[:, :, None] - key_gates.T[:, None, :]
    key_positions = key_first + jnp.arange(span_rows)
    allowed = token_positions[:, None] >= key_positions[None, :]
    scores = jnp.where(allowed[None], scores, -1e30)
    new_peak = jnp.maximum(running_peak, jnp.max(scores, axis=-1))
    factor = jnp.exp(running_peak - new_peak)
    weights = jnp.where(allowed[None], jnp.exp(scores - new_peak[:, :, None]), 0.0)
    weight_sum = weight_sum * factor + jnp.sum(weights, axis=-1)
    update = jnp.einsum(
        "hqk,khd->qhd",
        weights.astype(jnp.bfloat16),
        value_heads,
        preferred_element_type=jnp.float32,
    )
    weighted = weighted * factor.T[:, :, None] + update
    return (new_peak, weight_sum, weighted)


def per_device(
    query_small,
    key_small,
    value_small,
    gates_small,
    query_large,
    key_large,
    value_large,
    gates_large,
    residual,
    mixer_small,
    mixer_large,
    mix_gain,
    value_weight,
    gate_weight,
    value_taps,
    gate_taps,
    down_weight,
    final_gain,
):
    shard_rows = query_small.shape[0]
    first_row = lax.axis_index("sp") * shard_rows
    token_positions = first_row + jnp.arange(shard_rows)
    last_position = first_row + shard_rows - 1
    whole_value, whole_gate, whole_down = gather_turned(
        (value_weight, gate_weight, down_weight), "sp", (0, 0, 1)
    )
    every_gate = (
        lax.all_gather(gates_small, "sp", axis=0, tiled=True),
        lax.all_gather(gates_large, "sp", axis=0, tiled=True),
    )
    heads_small = gates_small.shape[1]
    heads_large = gates_large.shape[1]

    def fresh(heads_here, head_dim):
        return (
            jnp.full((heads_here, shard_rows), -1e30, jnp.float32),
            jnp.zeros((heads_here, shard_rows), jnp.float32),
            jnp.zeros((shard_rows, heads_here, head_dim), jnp.float32),
        )

    pieces = sent_together((key_small, value_small, key_large, value_large), "sp", 0, 1)
    span_total = pieces[0].shape[0]
    block_rows = shard_rows * math.gcd(span_total // shard_rows, max(1, 1024 // shard_rows))

    def one_block(block_index, current):
        offset = block_index * block_rows
        sliced = [lax.dynamic_slice_in_dim(member, offset, block_rows, 0) for member in pieces]
        gate_small = lax.dynamic_slice_in_dim(every_gate[0], offset, block_rows, 0)
        gate_large = lax.dynamic_slice_in_dim(every_gate[1], offset, block_rows, 0)

        def update(previous):
            return (
                attend_block(
                    previous[0],
                    query_small,
                    gates_small,
                    sliced[0],
                    sliced[1],
                    gate_small,
                    token_positions,
                    offset,
                    DS,
                ),
                attend_block(
                    previous[1],
                    query_large,
                    gates_large,
                    sliced[2],
                    sliced[3],
                    gate_large,
                    token_positions,
                    offset,
                    DL,
                ),
            )

        def unchanged(previous):
            return previous

        return lax.cond(offset <= last_position, update, unchanged, current)

    block_count = span_total // block_rows
    small_state, large_state = lax.fori_loop(
        0, block_count, one_block, (fresh(heads_small, DS), fresh(heads_large, DL))
    )
    small_out = (
        (small_state[2] / small_state[1].T[:, :, None])
        .reshape(shard_rows, heads_small * DS)
        .astype(jnp.bfloat16)
    )
    large_out = (
        (large_state[2] / large_state[1].T[:, :, None])
        .reshape(shard_rows, heads_large * DL)
        .astype(jnp.bfloat16)
    )
    tensor_parts = lax.axis_size(TP)
    own_rows = shard_rows // tensor_parts
    joined = jnp.concatenate([small_out, large_out], axis=1)
    arrived = stepwise_exchange(joined, TP, (1, 0), 0, 1)
    layout = arrived.reshape(own_rows, tensor_parts, joined.shape[1])
    small_width = small_out.shape[1]
    all_small = layout[:, :, :small_width].reshape(own_rows, tensor_parts * small_width)
    all_large = layout[:, :, small_width:].reshape(own_rows, tensor_parts * large_out.shape[1])
    add_pieces = sent_together((mixer_small, mixer_large), TP, 0, 1)
    mix = jnp.dot(all_small, add_pieces[0], preferred_element_type=jnp.float32) + jnp.dot(
        all_large, add_pieces[1], preferred_element_type=jnp.float32
    )
    mixed = norm_rows(residual_scale * residual.astype(jnp.float32) + mix, mix_gain).astype(
        jnp.bfloat16
    )
    block_input = lax.all_gather(mixed, TP, axis=0, tiled=True)
    up_value = jnp.dot(block_input, whole_value, preferred_element_type=jnp.float32)
    up_gate = jnp.dot(block_input, whole_gate, preferred_element_type=jnp.float32)
    up_value = up_value.astype(jnp.bfloat16)
    up_gate = up_gate.astype(jnp.bfloat16)
    hidden_width = up_value.shape[1]
    trailing = jnp.concatenate([up_value[-2:], up_gate[-2:]], axis=1)
    earlier = passed_along(trailing, "sp", 1)
    padded_value = jnp.concatenate([earlier[:, :hidden_width], up_value], axis=0).astype(
        jnp.float32
    )
    padded_gate = jnp.concatenate([earlier[:, hidden_width:], up_gate], axis=0).astype(jnp.float32)
    filt_value = (
        value_taps[0] * padded_value[:-2]
        + value_taps[1] * padded_value[1:-1]
        + value_taps[2] * padded_value[2:]
    )
    filt_gate = (
        gate_taps[0] * padded_gate[:-2]
        + gate_taps[1] * padded_gate[1:-1]
        + gate_taps[2] * padded_gate[2:]
    )
    hidden = (jax.nn.silu(filt_gate) * filt_value).astype(jnp.bfloat16)
    ffn_terms = jnp.dot(hidden, whole_down, preferred_element_type=jnp.float32)
    ffn = lax.psum_scatter(
        ffn_terms.astype(jnp.bfloat16), TP, scatter_dimension=0, tiled=True
    ).astype(jnp.float32)
    return norm_rows(residual_scale * mixed.astype(jnp.float32) + ffn, final_gain).astype(
        jnp.bfloat16
    )


def solution(mesh):
    split = Mesh(mesh.devices.reshape(mesh.shape["sp"], 4, 2), ("sp", "tp_0", "tp_1"))
    placed = (
        P("sp", TP),
        P("sp", TP),
        P("sp", TP),
        P("sp", TP),
        P("sp", TP),
        P("sp", TP),
        P("sp", TP),
        P("sp", TP),
        P(SP_TP, None),
        P(TP, None),
        P(TP, None),
        P(),
        P("sp", TP),
        P("sp", TP),
        P(None, TP),
        P(None, TP),
        P(TP, "sp"),
        P(),
    )
    return jax.shard_map(
        per_device, mesh=split, in_specs=placed, out_specs=P(SP_TP, None), check_vma=False
    )
```

profile of v0, /device:TPU:1, one launch (start us, length us, event | category | flops | bytes accessed | tf_op | source)
XLA Modules:
  0.0 426.2 jit_solution(15232635295806895450)
XLA Ops:
  6.5 2.3 pad_maximum_fusion.1
  9.0 1.0 pad_maximum_fusion
  10.1 0.9 pad_maximum_fusion.2
  11.1 0.1 copy.44
  11.3 21.2 %all_gather.20 = f32[12288,1]{0,1:T(1,128)S(1)} all-gather(f32[768,1]{0,1:T(1,128)S(1)} %copy-done.9), channel_id=1, replica_groups=mesh['sp'=16,'tp_0'=4,'tp_1'=2] {'sp'}, dimensions={0}, use_global_device_ids=true | all-gather | bytes 52224 | tf_op jit(solution)/shard_map/all_gather | solution.py:146
  32.5 18.9 %all_gather.19 = f32[12288,2]{0,1:T(2,128)S(1)} all-gather(f32[768,2]{0,1:T(2,128)S(1)} %copy-done.3), channel_id=1, replica_groups=mesh['sp'=16,'tp_0'=4,'tp_1'=2] {'sp'}, dimensions={0}, use_global_device_ids=true | all-gather | bytes 104448 | tf_op jit(solution)/shard_map/all_gather | solution.py:145
  51.4 51.7 %all-gather.5.cloned.1.call-done = bf16[12288,512]{1,0:T(8,128)(2,1)} async-done(((bf16[768,512]{1,0:T(8,128)(2,1)}), bf16[12288,512]{1,0:T(8,128)(2,1)}) %all-gather.5.cloned.1.call-update) | async-done | bytes 12582928 | tf_op jit(solution)/shard_map/all_gather | solution.py:35
  103.2 8.7 %fusion.66 = (bf16[12288,128]{1,0:T(8,128)(2,1)}, bf16[12288,128]{1,0:T(8,128)(2,1)}, bf16[12288,128]{1,0:T(8,128)(2,1)S(1)}, bf16[12288,128]{1,0:T(8,128)(2,1)}) fusion(bf16[12288,512]{1,0:T(8,128)(2,1)} %all-gather.5.cloned.1.call-done), kind=kLoop, calls=%fused_computation.99 | loop fusion | bytes 25165824 | tf_op jit(solution)/shard_map/slice | solution.py:37
  111.8 4.8 %copy.43 = bf16[12288,128]{0,1:T(8,128)(2,1)} copy(bf16[12288,128]{1,0:T(8,128)(2,1)} %get-tuple-element.740) | data formatting | bytes 6291456
  116.6 2.9 copy.45
  119.6 12.4 %while.24 = (s32[]{:T(128)}, f32[2,768]{1,0:T(2,128)S(1)}, f32[2,768]{1,0:T(2,128)S(1)}, f32[768,2,64]{0,2,1:T(8,128)S(1)}, f32[1,768]{1,0:T(1,128)S(1)}, /*inde...) while((s32[]{:T(128)}, f32[2,768]{1,0:T(2,128)S(1)}, ...), condition=%wide.region_7.8_spmd.clone, body=%wide.region_0.7_spmd.clone.sunk | while | flops 640360704 | bytes 27399704 | solution.py:200
  119.6 11.4 %conditional.3 = ((f32[2,768]{1,0:T(2,128)S(1)}, f32[2,768]{1,0:T(2,128)S(1)}, f32[768,2,64]{0,2,1:T(8,128)S(1)}, f32[1,768]{1,0:T(1,128)S(1)}, f32[1,768]{1,0:T(1,128)S(1)}, /*index=5*/f32[768,1,128]{0,2,1:T(8,128)S(1)})) conditional(s32[]{:T(128)} %convert_element_type.124, (f32[2,768]{1,0:T(2,128)S(1)}, f32[2,768]{1,0:T(2,128)S(1)}, ...), branch_computations={%region_1.0_spmd, %region_2.6_spmd} | conditional | flops 640360704 | bytes 27396218 | solution.py:197
  119.7 1.7 fusion.8
  121.4 1.9 fusion.17
  123.4 0.8 fusion.10
  124.3 0.4 broadcast_compare_fusion
  124.7 1.2 constant_dynamic-slice_fusion
  125.8 1.5 fusion.4
  127.3 2.0 fusion.14
  129.3 1.7 fusion.3
  132.0 0.3 convert_element_type.69
  132.3 0.2 copy.46
  132.5 0.2 divide_convert_fusion
  132.7 0.2 copy.47
  132.9 0.8 pad_maximum_fusion.3
  133.7 0.5 copy.48
  134.2 4.4 %all_to_all.10 = bf16[4,2,96,256]{3,2,0,1:T(8,128)(2,1)S(1)} all-to-all(bf16[4,2,96,256]{3,2,0,1:T(8,128)(2,1)S(1)} %copy.48), channel_id=1, replica_groups=mesh['sp'=16,'tp_0'=4,'tp_1'=2] {'tp_1'}, dimensions={1} | all-to-all | bytes 786432 | tf_op jit(solution)/shard_map/all_to_all | solution.py:58
  138.7 16.5 %all_to_all.11 = bf16[4,2,96,256]{3,2,1,0:T(8,128)(2,1)S(1)} all-to-all(bf16[4,2,96,256]{3,2,1,0:T(8,128)(2,1)S(1)} %copy.49), channel_id=1, replica_groups=mesh['sp'=16,'tp_0'=4,'tp_1'=2] {'tp_0'}, dimensions={0} | all-to-all | bytes 786432 | tf_op jit(solution)/shard_map/all_to_all | solution.py:58
  155.2 0.2 copy.65
  155.5 3.5 all-gather.7.cloned.1.call-done
  159.0 3.0 fusion.32
  162.0 3.2 fusion.69
  165.2 0.2 multiply_reduce_fusion.1
  165.5 0.9 multiply_convert_fusion.1
  166.5 67.4 %all-gather.11.cloned.1.call-done = bf16[2048,2112]{0,1:T(8,128)(2,1)} async-done(((bf16[128,2112]{0,1:T(8,128)(2,1)}), bf16[2048,2112]{0,1:T(8,128)(2,1)}) %all-gather.11.cloned.1.call-update) | async-done | bytes 8650768 | tf_op jit(solution)/shard_map/all_gather | solution.py:23
  233.9 119.7 %all-gather.9.cloned.1.call-done = bf16[768,2048]{1,0:T(8,128)(2,1)} async-done(((bf16[96,2048]{1,0:T(8,128)(2,1)}), bf16[768,2048]{1,0:T(8,128)(2,1)}) %all-gather.9.cloned.1.call-update) | async-done | bytes 3145744 | tf_op jit(solution)/shard_map/all_gather | solution.py:228
  353.6 5.3 %fusion.53 = bf16[768,704]{0,1:T(8,128)(2,1)S(1)} fusion(bf16[768,2048]{1,0:T(8,128)(2,1)} %all-gather.9.cloned.1.call-done, bf16[2048,2112]{0,1:T(8,128)(2,1)} %all-gather.11.cloned.1.call-done), kind=kOutput, calls=%fused_computation.66 | convolution fusion | flops 2215133184 | bytes 7110656 | tf_op jit(solution)/shard_map/dot_general | solution.py:229
  359.1 0.6 copy-done.14
  359.8 2.5 fusion.56
  362.2 0.1 slice.105
  362.4 3.3 collective-permute-start
  365.9 7.1 %collective-permute-done = bf16[2,1408]{0,1:T(8,128)(2,1)S(1)} collective-permute-done((bf16[2,1408]{0,1:T(8,128)(2,1)S(1)}, bf16[2,1408]{0,1:T(8,128)(2,1)S(1)}, u32[]{:S(2)}, u32[]{:S(2)}) %collective-permute-start) | collective-permute-done | bytes 5664 | tf_op jit(solution)/shard_map/ppermute | solution.py:70
  373.0 1.1 maximum_convert_fusion
  374.1 7.0 %convolution_convert_fusion = bf16[768,2048]{1,0:T(8,128)(2,1)} fusion(bf16[2048,2112]{0,1:T(8,128)(2,1)S(1)} %copy-done.13, f32[770,704]{0,1:T(8,128)S(1)} %get-tuple-element.748, f32[770,704]{0,1:T(8,128)S(1)} %get-tuple-element.747, f32[704]{0:T(1024)S(1)} %get-tuple-element.686, f32[704]{0:T(1024)S(1)} %get-tuple-element.687, ...), kind=kOutput, calls=%fused_computation.46 | convolution fusion | flops 2224816128 | bytes 19030016 | tf_op jit(solution)/shard_map/dot_general | solution.py:251
  381.1 34.5 %reduce-scatter.2.cloned.1.call-done = bf16[96,2048]{1,0:T(8,128)(2,1)} async-done(((bf16[768,2048]{1,0:T(8,128)(2,1)}), bf16[96,2048]{1,0:T(8,128)(2,1)}) %reduce-scatter.2.cloned.1.call-update) | async-done | bytes 393232 | tf_op jit(solution)/shard_map/reduce_scatter | solution.py:252
  415.6 1.4 fusion.60
  417.0 1.4 multiply_reduce_fusion
  418.5 1.2 multiply_convert_fusion
  (100 shorter events, 1.2 us)
Async XLA Ops:
  6.5 2.5 copy-start.2
  6.5 2.5 copy-start.1
  6.5 96.6 %all-gather.5.cloned.1.call-start = ((), (), s32[]{:S(2)}) async-start(), calls=%async_computation.3 | async-start | bytes 13369344 | tf_op jit(solution)/shard_map/all_gather | solution.py:35
  8.9 1.2 copy-start.5
  8.9 1.2 copy-start.6
  8.9 1.2 copy-start.7
  8.9 2.2 copy-start.4
  8.9 2.4 copy-start.9
  8.9 23.6 %copy-start.3 = (f32[768,2]{0,1:T(2,128)S(1)}, f32[768,2]{0,1:T(2,128)}, u32[]{:S(2)}) copy-start(f32[768,2]{0,1:T(2,128)} %param.25) | copy-start | bytes 18436
  9.0 150.0 %all-gather.7.cloned.1.call-start = ((), (), s32[]{:S(2)}) async-start(), calls=%async_computation.4 | async-start | bytes 9437184 | tf_op jit(solution)/shard_map/all_gather | solution.py:35
  10.1 223.9 %all-gather.11.cloned.1.call-start = ((), (), s32[]{:S(2)}) async-start(), calls=%async_computation.6 | async-start | bytes 9191424 | tf_op jit(solution)/shard_map/all_gather | solution.py:23
  11.1 342.6 %all-gather.9.cloned.1.call-start = ((), (), s32[]{:S(2)}) async-start(), calls=%async_computation.5 | async-start | bytes 3538944 | tf_op jit(solution)/shard_map/all_gather | solution.py:228
  159.0 3.0 copy-start.15
  162.0 3.5 copy-start.8
  166.4 249.1 %reduce-scatter.2.cloned.1.call-start = ((), (), s32[]{:S(2)}) async-start(), calls=%async_computation.7 | async-start | bytes 3538944 | tf_op jit(solution)/shard_map/reduce_scatter | solution.py:252
  353.6 5.5 %copy-start.13 = (bf16[2048,2112]{0,1:T(8,128)(2,1)S(1)}, bf16[2048,2112]{0,1:T(8,128)(2,1)}, u32[]{:S(2)}) copy-start(bf16[2048,2112]{0,1:T(8,128)(2,1)} %all-gather.11.cloned.1.call-done) | copy-start | bytes 25952260
  353.6 6.1 %copy-start.14 = (bf16[768,2048]{1,0:T(8,128)(2,1)S(1)}, bf16[768,2048]{1,0:T(8,128)(2,1)}, u32[]{:S(2)}) copy-start(bf16[768,2048]{1,0:T(8,128)(2,1)} %all-gather.9.cloned.1.call-done) | copy-start | bytes 9437188
  359.8 6.0 %copy-start.11 = (f32[3,704]{1,0:T(4,128)S(1)}, f32[3,704]{1,0:T(4,128)}, u32[]{:S(2)}) copy-start(f32[3,704]{1,0:T(4,128)} %param.36) | copy-start | bytes 25348
  359.8 6.0 %copy-start.12 = (f32[3,704]{1,0:T(4,128)S(1)}, f32[3,704]{1,0:T(4,128)}, u32[]{:S(2)}) copy-start(f32[3,704]{1,0:T(4,128)} %param.37) | copy-start | bytes 25348
  362.4 10.6 %collective-permute-start = (bf16[2,1408]{0,1:T(8,128)(2,1)S(1)}, bf16[2,1408]{0,1:T(8,128)(2,1)S(1)}, u32[]{:S(2)}, u32[]{:S(2)}) collective-permute-start(bf16[2,1408]{0,1:T(8,128)(2,1)S(1)} %pad_maximum_fusion.4), channel_id=1, source_target_pairs={{0,8},{8,16},{16,24},{24,32},{32,40},{40,48},{48,56},{56,64},{64,7... | collective-permute-start | bytes 16904 | tf_op jit(solution)/shard_map/ppermute | solution.py:70
  381.1 37.4 %copy-start.10 = (f32[2048]{0:T(1024)S(1)}, f32[2048]{0:T(1024)}, u32[]{:S(2)}) copy-start(f32[2048]{0:T(1024)} %param.39) | copy-start | bytes 24580
  415.6 2.9 copy-start
Sparse Core Ops, SparseCore 0:
  9.5 93.6 all-gather.4
  104.9 54.0 all-gather.6
  161.1 72.7 all-gather.10
  235.5 118.1 all-gather.8
  381.2 34.3 reduce-scatter.1
where the time goes:
time: 430 us; the launch traced here: 426 us
  waiting for transfers between devices  284 us (66%)
  blocking collectives  61.1 us (14%)
  matrix products  28.1 us (7%)
  local copies, waits for them, and re-layouts  20.2 us (5%)
  other arithmetic  14.6 us (3%)
  between operations  13.5 us (3%)
    all_gather x1, waiting for transfers between devices, per_device(): block_input = lax.all_gather(mixed, TP, axis=0, tiled=True)  120 us
    all_gather x1, waiting for transfers between devices, gather_turned(): out = lax.all_gather(both, axis, axis=0, tiled=True)  67.4 us
    all_gather x2, waiting for transfers between devices, sent_together(): lax.all_gather(both, axis, axis=dim, tiled=True)  55.2 us
    reduce_scatter x1, waiting for transfers between devices, per_device(): lax.psum_scatter(ffn_terms.astype(jnp.bfloat16), TP, scatter_dimension=0,...  34.5 us
    all_gather x1, blocking collectives, per_device(): lax.all_gather(gates_large, 'sp', axis=0, tiled=True)  21.2 us
    all_to_all x2, blocking collectives, moved_by_axis(): lax.all_to_all(pieces, axes[k], split_axis=k, concat_axis=k, tiled=True)  21 us
    all_gather x1, blocking collectives, per_device(): lax.all_gather(gates_small, 'sp', axis=0, tiled=True)  18.9 us
    slice x1, local copies, waits for them, and re-layouts, sent_together(): finished.append(lax.slice_in_dim(out, at, at + a.shape[along], axis=along))  8.66 us
  transfers between devices with their start and end apart: 6, of which 6 were waited for; matrix products, arithmetic and copies ran while one was open for 9% of the time, Pallas kernels for 0%

commit v1 on v0

v1 whole, which is shorter than its diff:
```python
import functools

import jax
import jax.numpy as jnp
from jax import lax
from jax.experimental import pallas as pl
from jax.experimental.pallas import tpu as pltpu
from jax.sharding import Mesh
from jax.sharding import PartitionSpec as P

TP = ("tp_0", "tp_1")
SP_TP = ("sp", "tp_0", "tp_1")
LOG2E = 1.4426950408889634
residual_scale = 2.0**0.5
epsilon = 1e-05
MESH = pl.DeviceIdType.MESH
BLK = 768
EXTRA = 32
RQ = 256
F32 = jnp.float32
BF16 = jnp.bfloat16
VMEM_ALL = 60 * 1024 * 1024


def gather_attend(
    kv_ref,
    q_ref,
    up_ref,
    down_ref,
    mix_ref,
    att_ref,
    up_all,
    down_all,
    mix_all,
    kvbuf,
    qpair,
    qm,
    gq,
    gk,
    mst,
    lst,
    acc,
    outv,
    ssem,
    rsem,
    lsem,
):
    sp = lax.axis_index("sp")
    y = lax.axis_index("tp_0")
    c = lax.axis_index("tp_1")
    z, x = sp // 4, sp % 4
    role = x // 2
    xr, xl = (x + 1) % 4, (x + 3) % 4
    zu, zd = (z + 1) % 4, (z + 3) % 4
    yu, yd = (y + 1) % 4, (y + 3) % 4
    zf, yf = (z + 2) % 4, (y + 2) % 4
    mate = x + 1 - 2 * (x % 2)
    opp = 3 - x
    diag = opp + 1 - 2 * (opp % 2)
    pair_sp = 15 - sp

    def at(zz, xx):
        return (zz * 4 + xx, y, c)

    right, left = at(z, xr), at(z, xl)
    above, below = at(zu, x), at(zd, x)
    mate_dev, opp_dev = at(z, mate), at(z, opp)
    pair_dev = (pair_sp, y, c)
    y_up, y_down = (sp, yu, c), (sp, yd, c)
    sibling = (sp, y, 1 - c)
    tp = y * 2 + c

    barrier = pltpu.get_barrier_semaphore()
    for dev in (right, left, above, below, pair_dev, y_up, y_down, sibling):
        pl.semaphore_signal(barrier, inc=1, device_id=dev, device_id_type=MESH)
    pl.semaphore_wait(barrier, 8)

    sent = []
    counter = [0]
    incoming = {}

    def send(name, src, dst, dev, landing):
        k = counter[0]
        counter[0] += 1
        copy = pltpu.make_async_remote_copy(
            src_ref=src,
            dst_ref=dst,
            send_sem=ssem.at[k],
            recv_sem=rsem.at[k],
            device_id=dev,
            device_id_type=MESH,
        )
        copy.start()
        sent.append(copy)
        incoming[name] = pltpu.make_async_remote_copy(
            src_ref=landing,
            dst_ref=landing,
            send_sem=ssem.at[k],
            recv_sem=rsem.at[k],
            device_id=dev,
            device_id_type=MESH,
        )

    def take(*names):
        for name in names:
            incoming.pop(name).wait_recv()

    cols = {"own": x, "mate": mate, "opp": opp, "diag": diag}

    send("x1m", kv_ref.at[role], kvbuf.at[sp], mate_dev, kvbuf.at[z * 4 + mate])
    send("x1o", kv_ref.at[1 - role], kvbuf.at[sp], opp_dev, kvbuf.at[z * 4 + opp])
    send("wz1u_up", up_ref, up_all.at[sp], above, up_all.at[zd * 4 + x])
    send("wz1d_up", up_ref, up_all.at[sp], below, up_all.at[zu * 4 + x])
    send("wz1u_dn", down_ref, down_all.at[sp], above, down_all.at[zd * 4 + x])
    send("wz1d_dn", down_ref, down_all.at[sp], below, down_all.at[zu * 4 + x])
    send("q", q_ref.at[1 - role], qpair, pair_dev, qpair)
    send("z1u_own", kv_ref.at[role], kvbuf.at[sp], above, kvbuf.at[zd * 4 + x])
    send("z1d_own", kv_ref.at[role], kvbuf.at[sp], below, kvbuf.at[zu * 4 + x])
    send("y1u", mix_ref, mix_all.at[tp], y_up, mix_all.at[yd * 2 + c])
    send("y1d", mix_ref, mix_all.at[tp], y_down, mix_all.at[yu * 2 + c])
    send("s0", mix_ref, mix_all.at[tp], sibling, mix_all.at[y * 2 + 1 - c])

    def pass_x(tag, zz, up_src, down_src):
        row = zz * 4
        send("wx1r_up" + tag, up_src, up_all.at[row + x], right, up_all.at[row + xl])
        send("wx1l_up" + tag, up_src, up_all.at[row + x], left, up_all.at[row + xr])
        send("wx1r_dn" + tag, down_src, down_all.at[row + x], right, down_all.at[row + xl])
        send("wx1l_dn" + tag, down_src, down_all.at[row + x], left, down_all.at[row + xr])

    pass_x("0", z, up_ref, down_ref)

    locals_ = [
        pltpu.make_async_copy(kv_ref.at[role], kvbuf.at[sp], lsem.at[0]),
        pltpu.make_async_copy(up_ref, up_all.at[sp], lsem.at[1]),
        pltpu.make_async_copy(down_ref, down_all.at[sp], lsem.at[2]),
        pltpu.make_async_copy(mix_ref, mix_all.at[tp], lsem.at[3]),
    ]
    for copy in locals_:
        copy.start()

    heads = 2 - role
    head_dim = 64 + 64 * role
    scale = jnp.where(role == 0, 0.125 * LOG2E, 128.0**-0.5 * LOG2E).astype(F32)
    lane = lax.broadcasted_iota(jnp.int32, (1, 128), 1)

    def head_lanes(h):
        return (lane >= h * 64) & (lane < h * 64 + head_dim)

    def load_queries(qi, ref):
        packed = ref[:, 128:256].astype(F32)
        for h in range(2):
            keep = jnp.where(head_lanes(h), 1.0, 0.0).astype(BF16)
            qm[qi, h] = ref[:, 0:128] * keep
            mine = (lane >= 3 * h) & (lane < 3 * h + 3)
            total = jnp.sum(jnp.where(mine, packed, 0.0), axis=1, keepdims=True)
            gq[qi, h] = jnp.broadcast_to(total, (BLK, 128))

    load_queries(0, q_ref.at[role])
    mst[...] = jnp.full(mst.shape, -1e30, F32)
    lst[...] = jnp.zeros(lst.shape, F32)
    acc[...] = jnp.zeros(acc.shape, F32)

    def pass_z(tag):
        col = cols[tag]
        send("z1u_" + tag, kvbuf.at[z * 4 + col], kvbuf.at[z * 4 + col], above, kvbuf.at[zd * 4 + col])
        send("z1d_" + tag, kvbuf.at[z * 4 + col], kvbuf.at[z * 4 + col], below, kvbuf.at[zu * 4 + col])

    take("x1o")
    send("x2", kvbuf.at[z * 4 + opp], kvbuf.at[z * 4 + opp], mate_dev, kvbuf.at[z * 4 + diag])
    take("x1m")
    take("wz1u_up", "wz1d_up", "wz1u_dn", "wz1d_dn")
    b_d, b_u, b_f = zd * 4 + x, zu * 4 + x, zf * 4 + x
    top, rest = pl.ds(0, 96), pl.ds(96, 32)
    send("wz2u", up_all.at[b_d, top], up_all.at[b_d, top], above, up_all.at[b_f, top])
    send("wz2d", up_all.at[b_u, rest], up_all.at[b_u, rest], below, up_all.at[b_f, rest])
    send("wz2dd", down_all.at[b_u], down_all.at[b_u], below, down_all.at[b_f])
    pass_z("mate")
    pass_z("opp")
    pass_x("d", zd, up_all.at[b_d], down_all.at[b_d])
    pass_x("u", zu, up_all.at[b_u], down_all.at[b_u])
    take("x2")
    pass_z("diag")
    take("q")
    load_queries(1, qpair)
    take("wz2u", "wz2d", "wz2dd")
    pass_x("f", zf, up_all.at[b_f], down_all.at[b_f])
    locals_[0].wait()

    def gate_rows(j):
        rows = kvbuf[j, BLK : BLK + EXTRA, :].astype(F32)
        for h in range(2):
            for p in range(3):
                k = h * 9 + p
                g = rows[k : k + 1] + rows[k + 3 : k + 4] + rows[k + 6 : k + 7]
                gk[j * 2 + h, :, p * 256 : (p + 1) * 256] = jnp.broadcast_to(g, (8, 256))

    def tile(qi, qblk, j, h, sub, masked):
        r0 = pl.multiple_of(sub * RQ, RQ)
        rows = pl.ds(r0, RQ)
        keep = head_lanes(h)
        q = qm[qi, h, rows, :]
        s = lax.dot_general(
            q, kvbuf[j, 0:BLK, 0:128], (((1,), (1,)), ((), ())), preferred_element_type=F32
        )
        gate = gk[j * 2 + h, 0:1, :]
        parts = []
        for g in range(BLK // 128):
            part = s[:, g * 128 : (g + 1) * 128] * scale - gate[:, g * 128 : (g + 1) * 128]
            if masked:
                col = lax.broadcasted_iota(jnp.int32, (RQ, 128), 1) + g * 128
                row = lax.broadcasted_iota(jnp.int32, (RQ, 128), 0) + sub * RQ
                part = jnp.where(col <= row, part, -1e30)
            parts.append(part)
        peak = functools.reduce(jnp.maximum, parts)
        peak = jnp.max(peak, axis=1, keepdims=True)
        g_here = gq[qi, h, rows, :]
        old = mst[qi, h, rows, :]
        new = jnp.maximum(old, peak + g_here)
        alpha = jnp.exp2(old - new)
        shift = new - g_here
        weights = [jnp.exp2(part - shift) for part in parts]
        mst[qi, h, rows, :] = new
        lst[qi, h, rows, :] = lst[qi, h, rows, :] * alpha + functools.reduce(jnp.add, weights)
        w = jnp.concatenate([a.astype(BF16) for a in weights], axis=1)
        v = kvbuf[j, 0:BLK, 128:256] * jnp.where(keep, 1.0, 0.0).astype(BF16)
        update = jnp.dot(w, v, preferred_element_type=F32)
        acc[qi, rows, :] = acc[qi, rows, :] * jnp.where(keep, alpha, 1.0) + update

    def attend_row(zz):
        for xx in range(4):
            gate_rows(zz * 4 + xx)

        def for_queries(qi, _):
            qblk = jnp.where(qi == 0, sp, pair_sp)
            full = jnp.clip(qblk - 4 * zz, 0, 4)

            def for_block(jj, _):
                def for_head(h, _):
                    def for_rows(sub, _):
                        tile(qi, qblk, zz * 4 + jj, h, sub, False)
                        return 0

                    return lax.fori_loop(0, BLK // RQ, for_rows, 0)

                return lax.fori_loop(0, heads, for_head, 0)

            lax.fori_loop(0, full, for_block, 0)

            @pl.when(qblk // 4 == zz)
            def _():
                def for_head(h, _):
                    def for_rows(sub, _):
                        tile(qi, qblk, qblk, h, sub, True)
                        return 0

                    return lax.fori_loop(0, BLK // RQ, for_rows, 0)

                lax.fori_loop(0, heads, for_head, 0)

            return 0

        lax.fori_loop(0, 2, for_queries, 0)

    attend_row(z)

    def pass_on(tag, name, from_z, dev, landing_z):
        col = cols[tag]
        src = kvbuf.at[from_z * 4 + col]
        send(name + tag, src, src, dev, kvbuf.at[landing_z * 4 + col])

    take("z1u_own", "z1d_own", "z1u_mate", "z1d_mate")
    pass_on("own", "z2u_", zd, above, zf)
    pass_on("mate", "z2u_", zd, above, zf)
    take("z1u_opp", "z1d_opp", "z1u_diag", "z1d_diag")
    pass_on("opp", "z2d_", zu, below, zf)
    pass_on("diag", "z2d_", zu, below, zf)

    take("y1u", "y1d")
    m_d, m_u, m_f = yd * 2 + c, yu * 2 + c, yf * 2 + c
    s_d, s_u, s_f = yd * 2 + 1 - c, yu * 2 + 1 - c, yf * 2 + 1 - c
    first, second = pl.ds(0, 128), pl.ds(128, 128)
    send("y2u", mix_all.at[m_d, first], mix_all.at[m_d, first], y_up, mix_all.at[m_f, first])
    send("y2d", mix_all.at[m_u, second], mix_all.at[m_u, second], y_down, mix_all.at[m_f, second])
    send("s1", mix_all.at[m_d], mix_all.at[m_d], sibling, mix_all.at[s_d])
    send("s2", mix_all.at[m_u], mix_all.at[m_u], sibling, mix_all.at[s_u])

    attend_row(zd)

    def pass_x2(tag, zz, name, col, dev, landing):
        for kind, whole in (("_up", up_all), ("_dn", down_all)):
            src = whole.at[zz * 4 + col]
            send(name + kind + tag, src, src, dev, whole.at[zz * 4 + landing])

    xf = (x + 2) % 4
    for tag in ("0", "d"):
        take("wx1r_up" + tag, "wx1r_dn" + tag, "wx1l_up" + tag, "wx1l_dn" + tag)
    pass_x2("0", z, "wx2r", xl, right, xf)
    pass_x2("d", zd, "wx2r", xl, right, xf)

    attend_row(zu)

    for tag in ("u", "f"):
        take("wx1r_up" + tag, "wx1r_dn" + tag, "wx1l_up" + tag, "wx1l_dn" + tag)
    pass_x2("u", zu, "wx2l", xr, left, xf)
    pass_x2("f", zf, "wx2l", xr, left, xf)
    take("y2u", "y2d")
    send("s3", mix_all.at[m_f], mix_all.at[m_f], sibling, mix_all.at[s_f])
    take("z2u_own", "z2u_mate", "z2d_opp", "z2d_diag")

    attend_row(zf)

    keep0 = head_lanes(0)
    for qi in (1, 0):
        l0 = jnp.sum(lst[qi, 0], axis=1, keepdims=True)
        l1 = jnp.sum(lst[qi, 1], axis=1, keepdims=True)
        outv[qi] = (acc[qi] / jnp.where(keep0, l0, l1)).astype(BF16)
    send("out", outv.at[1], att_ref.at[role], pair_dev, att_ref.at[1 - role])
    own_out = pltpu.make_async_copy(outv.at[0], att_ref.at[role], lsem.at[4])
    own_out.start()
    take(*list(incoming))
    own_out.wait()
    for copy in locals_[1:]:
        copy.wait()
    for copy in sent:
        copy.wait_send()


def gather_and_attend(kv, q, up, down, mixers):
    any_ = pl.BlockSpec(memory_space=pl.ANY)
    vmem = pl.BlockSpec(memory_space=pltpu.VMEM)
    return pl.pallas_call(
        gather_attend,
        out_shape=(
            jax.ShapeDtypeStruct((2, BLK, 128), BF16),
            jax.ShapeDtypeStruct((16, *up.shape), BF16),
            jax.ShapeDtypeStruct((16, *down.shape), BF16),
            jax.ShapeDtypeStruct((8, *mixers.shape), BF16),
        ),
        in_specs=[vmem] * 5,
        out_specs=(any_,) * 4,
        scratch_shapes=[
            pltpu.VMEM((16, BLK + EXTRA, 256), BF16),
            pltpu.VMEM((BLK, 256), BF16),
            pltpu.VMEM((2, 2, BLK, 128), BF16),
            pltpu.VMEM((2, 2, BLK, 128), F32),
            pltpu.VMEM((32, 8, BLK), F32),
            pltpu.VMEM((2, 2, BLK, 128), F32),
            pltpu.VMEM((2, 2, BLK, 128), F32),
            pltpu.VMEM((2, BLK, 128), F32),
            pltpu.VMEM((2, BLK, 128), BF16),
            pltpu.SemaphoreType.DMA((72,)),
            pltpu.SemaphoreType.DMA((72,)),
            pltpu.SemaphoreType.DMA((8,)),
        ],
        compiler_params=pltpu.CompilerParams(
            collective_id=1, has_side_effects=True, vmem_limit_bytes=VMEM_ALL
        ),
        cost_estimate=pl.CostEstimate(flops=20_000_000_000, bytes_accessed=40_000_000, transcendentals=0),
    )(kv, q, up, down, mixers)


def three_parts(gates):
    scaled = gates * LOG2E
    high = lax.reduce_precision(scaled, 8, 7)
    middle = lax.reduce_precision(scaled - high, 8, 7)
    low = lax.reduce_precision(scaled - high - middle, 8, 7)
    return jnp.stack([high, middle, low], axis=1).astype(BF16)


def packed_inputs(query, keys, values, gates):
    rows = keys.shape[0]
    parts = three_parts(gates)
    heads = gates.shape[1]
    by_lane = parts.transpose(2, 1, 0).reshape(heads * 9, 256)
    by_lane = jnp.pad(by_lane, ((0, EXTRA - heads * 9), (0, 0)))
    kv = jnp.concatenate([jnp.concatenate([keys, values], axis=1), by_lane], axis=0)
    by_row = parts.transpose(0, 2, 1).reshape(rows, heads * 3)
    by_row = jnp.pad(by_row, ((0, 0), (0, 128 - heads * 3)))
    return kv, jnp.concatenate([query, by_row], axis=1)


def split_up(array, dim, devices):
    shape = array.shape
    pieces = array.reshape(*shape[:dim], devices, shape[dim] // devices, *shape[dim + 1 :])
    return jnp.moveaxis(pieces, dim, 0)


def laid_out(pieces, dim):
    shape = list(pieces.shape[1:])
    shape[dim] *= pieces.shape[0]
    return jnp.moveaxis(pieces, 0, dim).reshape(shape)


def moved_by_axis(pieces, axes, turns):
    shape = [lax.axis_size(a) for a in axes]
    pieces = pieces.reshape(*shape, *pieces.shape[1:])
    for k in turns:
        pieces = lax.all_to_all(pieces, axes[k], split_axis=k, concat_axis=k, tiled=True)
    return pieces.reshape(-1, *pieces.shape[len(axes) :])


def stepwise_exchange(array, axes, turns, split_dim, concat_dim):
    pieces = split_up(array, split_dim, lax.axis_size(axes))
    return laid_out(moved_by_axis(pieces, axes, turns), concat_dim)


def passed_along(value, axis, steps):
    count = lax.axis_size(axis)
    first, last = (max(0, -steps), min(count, count - steps))
    return lax.ppermute(value, axis, [(source, source + steps) for source in range(first, last)])


def norm_rows(values, gain):
    center = jnp.mean(values, axis=-1, keepdims=True)
    spread = jnp.mean(jnp.square(values - center), axis=-1, keepdims=True)
    return (values - center) * lax.rsqrt(spread + epsilon) * gain


def per_device(
    query_small,
    key_small,
    value_small,
    gates_small,
    query_large,
    key_large,
    value_large,
    gates_large,
    residual,
    mixer_small,
    mixer_large,
    mix_gain,
    value_weight,
    gate_weight,
    value_taps,
    gate_taps,
    down_weight,
    final_gain,
):
    shard_rows = query_small.shape[0]
    kv_s, q_s = packed_inputs(query_small, key_small, value_small, gates_small)
    kv_l, q_l = packed_inputs(query_large, key_large, value_large, gates_large)
    up = jnp.concatenate(
        [value_weight[:, :640], gate_weight[:, :640], value_weight[:, 640:], gate_weight[:, 640:]],
        axis=1,
    )
    mixers = jnp.concatenate([mixer_small, mixer_large], axis=0)
    att, up_all, down_all, mix_all = gather_and_attend(
        jnp.stack([kv_s, kv_l]), jnp.stack([q_s, q_l]), up, down_weight, mixers
    )
    up_all = up_all.reshape(-1, up_all.shape[2])
    mix_all = mix_all.reshape(-1, mix_all.shape[2])
    joined = jnp.concatenate([att[0], att[1]], axis=1)
    tensor_parts = lax.axis_size(TP)
    own_rows = shard_rows // tensor_parts
    arrived = stepwise_exchange(joined, TP, (1, 0), 0, 1)
    mix = jnp.dot(arrived.reshape(own_rows, -1), mix_all, preferred_element_type=jnp.float32)
    mixed = norm_rows(residual_scale * residual.astype(jnp.float32) + mix, mix_gain).astype(
        jnp.bfloat16
    )
    block_input = lax.all_gather(mixed, TP, axis=0, tiled=True)
    both = jnp.dot(block_input, up_all, preferred_element_type=jnp.float32).astype(jnp.bfloat16)
    taps = jnp.concatenate(
        [value_taps[:, :640], gate_taps[:, :640], value_taps[:, 640:], gate_taps[:, 640:]], axis=1
    )
    earlier = passed_along(both[-2:], "sp", 1)
    padded = jnp.concatenate([earlier, both], axis=0).astype(jnp.float32)
    filt = taps[0] * padded[:-2] + taps[1] * padded[1:-1] + taps[2] * padded[2:]
    filt_value = jnp.concatenate([filt[:, :640], filt[:, 1280:1344]], axis=1)
    filt_gate = jnp.concatenate([filt[:, 640:1280], filt[:, 1344:]], axis=1)
    hidden = (jax.nn.silu(filt_gate) * filt_value).astype(jnp.bfloat16)
    whole_down = down_all.transpose(1, 0, 2).reshape(down_all.shape[1], -1)
    ffn_terms = jnp.dot(hidden, whole_down, preferred_element_type=jnp.float32)
    ffn = lax.psum_scatter(
        ffn_terms.astype(jnp.bfloat16), TP, scatter_dimension=0, tiled=True
    ).astype(jnp.float32)
    return norm_rows(residual_scale * mixed.astype(jnp.float32) + ffn, final_gain).astype(
        jnp.bfloat16
    )


def solution(mesh):
    split = Mesh(mesh.devices.reshape(mesh.shape["sp"], 4, 2), ("sp", "tp_0", "tp_1"))
    placed = (
        P("sp", TP),
        P("sp", TP),
        P("sp", TP),
        P("sp", TP),
        P("sp", TP),
        P("sp", TP),
        P("sp", TP),
        P("sp", TP),
        P(SP_TP, None),
        P(TP, None),
        P(TP, None),
        P(),
        P("sp", TP),
        P("sp", TP),
        P(None, TP),
        P(None, TP),
        P(TP, "sp"),
        P(),
    )
    return jax.shard_map(
        per_device, mesh=split, in_specs=placed, out_specs=P(SP_TP, None), check_vma=False
    )
```

time: 430 us -> 283 us (0.66)
  waiting for transfers between devices: 284 us -> 78.9 us
  Pallas kernels: 0 us -> 127 us
  blocking collectives: 61.1 us -> 17.7 us
  local copies, waits for them, and re-layouts: 20.2 us -> 8.3 us
  matrix products: 28.1 us -> 17.5 us
    pallas_call x0 -> x1, Pallas kernels: none -> 127 us  [gather_and_attend(): pl.pallas_call(gather_attend, out_shape=(jax.ShapeDtypeStruct((2, BLK, 12...]
    all_gather x3 -> x0, waiting for transfers between devices: 123 us -> none  [the longest x1 67.4 us: gather_turned(): out = lax.all_gather(both, axis, axis=0, tiled=True)]
    all_gather x1, waiting for transfers between devices: 120 us -> 43.8 us  [per_device(): block_input = lax.all_gather(mixed, TP, axis=0, tiled=True)]
    all_gather x2 -> x0, blocking collectives: 40.1 us -> none  [the longest x1 21.2 us: per_device(): lax.all_gather(gates_large, 'sp', axis=0, tiled=True)]
    dot_general x8 -> x2, matrix products: 21.1 us -> 13.4 us  [the longest x1 8.34 us: per_device(): jnp.dot(block_input, up_all, preferred_element_type=jnp.float32)]
    unnamed x35 -> x24, local copies, waits for them, and re-layouts: 8.49 us -> 1.97 us
    ppermute x1, waiting for transfers between devices: 7.15 us -> 0.7 us  [passed_along(): lax.ppermute(value, axis, [(source, source + steps) for source in range(f...]
    another operation x1 -> x7, other arithmetic: 0.02 us -> 4.77 us  [the longest x2 2.21 us: per_device(): jnp.stack([q_s, q_l])]
  transfers between devices with their start and end apart: 6 -> 3, of which waited for: 6 -> 3; matrix products, arithmetic and copies ran while one was open for 9% -> 0% of each run, Pallas kernels for 0% -> 0%
where the time goes in v1:
time: 283 us; the launch traced here: 280 us
  Pallas kernels  127 us (45%)
  waiting for transfers between devices  78.9 us (28%)
  blocking collectives  17.7 us (6%)
  matrix products  17.5 us (6%)
  other arithmetic  13.8 us (5%)
  between operations  13.7 us (5%)
  local copies, waits for them, and re-layouts  8.3 us (3%)
  starting transfers between devices  3.35 us (1%)
    pallas_call x1, Pallas kernels, gather_and_attend(): pl.pallas_call(gather_attend, out_shape=(jax.ShapeDtypeStruct((2, BLK, 12...  127 us
    all_gather x1, waiting for transfers between devices, per_device(): block_input = lax.all_gather(mixed, TP, axis=0, tiled=True)  43.8 us
    reduce_scatter x1, waiting for transfers between devices, per_device(): lax.psum_scatter(ffn_terms.astype(jnp.bfloat16), TP, scatter_dimension=0,...  34.3 us
    all_to_all x2, blocking collectives, moved_by_axis(): lax.all_to_all(pieces, axes[k], split_axis=k, concat_axis=k, tiled=True)  17.7 us
    dot_general x1, matrix products, per_device(): jnp.dot(block_input, up_all, preferred_element_type=jnp.float32)  8.34 us
  transfers between devices with their start and end apart: 3, of which 3 were waited for; matrix products, arithmetic and copies ran while one was open for 0% of the time, Pallas kernels for 0%

profile of v1, /device:TPU:1, one launch (start us, length us, event | category | flops | bytes accessed | tf_op | source)
XLA Modules:
  0.0 280.3 jit_solution(13564186520546596370)
XLA Ops:
  6.5 0.0 all-gather.2.cloned.1.call-start
  6.6 0.8 fusion.26
  7.4 0.9 slice.63
  8.3 0.7 slice.65
  9.1 0.9 slice.64
  10.0 0.7 slice.66
  10.7 0.7 reduce-precision_convert_fusion.3
  11.4 0.2 copy.65
  11.7 0.2 copy.64
  12.0 0.2 copy.75
  12.1 0.2 copy.76
  12.3 0.1 copy.77
  12.4 0.1 copy.78
  12.5 0.0 copy-start.1
  12.5 1.3 fusion.18
  13.8 1.0 pad_maximum_fusion.3.q_ref
  14.8 0.1 fusion.14
  14.9 1.0 pad_maximum_fusion.2.kv_ref
  15.9 1.1 pad_maximum_fusion.1.mix_ref
  17.0 0.8 concatenate.61.up_ref
  17.8 127.0 %shard_map.172 = (bf16[2,768,128]{2,1,0:T(8,128)(2,1)}, bf16[16,128,1408]{2,1,0:T(8,128)(2,1)}, bf16[16,704,128]{2,1,0:T(8,128)(2,1)}, bf16[8,256,2048]{2,1,0:T(8,128)(2,1)}) custom-call(bf16[2,800,256]{2,1,0:T(8,128)(2,1)} %pad_maximum_fusion.2.kv_ref, bf16[2,768,256]{2,1,0:T(8,128)(2,1)} %pad_maximum_fusion.3.q_ref, bf16[128,1408]{1,0:T(8,128)(2,1)} %concatenate.61.up_ref, ...), custom_call_target="tpu_custom_call" | custom-call | flops 20000000000 | bytes 40000000 | tf_op jit(solution)/shard_map/pallas_call | solution.py:331
  144.8 0.0 copy-start.2
  144.8 1.1 fusion.34
  146.0 6.8 %all_to_all.10 = bf16[4,2,96,256]{3,2,0,1:T(8,128)(2,1)S(1)} all-to-all(bf16[4,2,96,256]{3,2,0,1:T(8,128)(2,1)S(1)} %copy.74), channel_id=1, replica_groups=mesh['sp'=16,'tp_0'=4,'tp_1'=2] {'tp_1'}, dimensions={1} | all-to-all | bytes 786432 | tf_op jit(solution)/shard_map/all_to_all | solution.py:398
  152.8 10.9 %all_to_all.11 = bf16[4,2,96,256]{3,2,1,0:T(8,128)(2,1)S(1)} all-to-all(bf16[4,2,96,256]{3,2,1,0:T(8,128)(2,1)S(1)} %copy.72), channel_id=1, replica_groups=mesh['sp'=16,'tp_0'=4,'tp_1'=2] {'tp_0'}, dimensions={0} | all-to-all | bytes 786432 | tf_op jit(solution)/shard_map/all_to_all | solution.py:398
  163.8 0.0 slice-start.2
  163.8 5.0 %fusion.35 = (f32[96]{0:T(128)S(1)}, f32[96,2048]{1,0:T(8,128)S(1)}) fusion(bf16[96,8,256]{2,0,1:T(8,128)(2,1)S(1)} %bitcast.50, bf16[8,256,2048]{2,1,0:T(8,128)(2,1)} %get-tuple-element.10, bf16[96,2048]{1,0:T(8,128)(2,1)S(1)} %copy-done.2), kind=kOutput, calls=%fused_computation.72 | convolution fusion | flops 806092672 | bytes 9961856 | tf_op jit(solution)/shard_map/dot_general | solution.py:456
  168.9 0.2 multiply_reduce_fusion.1
  169.2 0.9 multiply_convert_fusion.1
  170.1 0.0 all-gather.2.cloned.1.call-update
  170.1 0.0 reduce-scatter.2.cloned.1.call-start
  170.2 0.1 concatenate.66
  170.3 43.8 %all-gather.2.cloned.1.call-done = bf16[768,2048]{1,0:T(8,128)(2,1)} async-done(((bf16[96,2048]{1,0:T(8,128)(2,1)}), bf16[768,2048]{1,0:T(8,128)(2,1)}) %all-gather.2.cloned.1.call-update) | async-done | bytes 3145744 | tf_op jit(solution)/shard_map/all_gather | solution.py:460
  214.1 8.3 %convolution_convert_fusion.1 = bf16[768,1408]{1,0:T(8,128)(2,1)S(1)} fusion(bf16[768,2048]{1,0:T(8,128)(2,1)} %all-gather.2.cloned.1.call-done, bf16[2048,1408]{1,0:T(8,128)(2,1)} %bitcast.55), kind=kOutput, calls=%fused_computation.6 | convolution fusion | flops 4430266368 | bytes 11075584 | tf_op jit(solution)/shard_map/dot_general | solution.py:461
  222.5 3.3 %collective-permute-start = (bf16[2,1408]{1,0:T(2,128)(2,1)S(1)}, bf16[2,1408]{1,0:T(2,128)(2,1)S(1)}, u32[]{:S(2)}, u32[]{:S(2)}) collective-permute-start(bf16[2,1408]{1,0:T(2,128)(2,1)S(1)} %slice.85), channel_id=1, source_target_pairs={{0,8},{8,16},{16,24},{24,32},{32,40},{40,48},{48,56},{56,64},{64,7... | collective-permute-start | bytes 16904 | tf_op jit(solution)/shard_map/ppermute | solution.py:410
  225.8 0.1 slice_reduce_fusion.2
  225.8 0.7 collective-permute-done
  226.5 0.4 maximum_convert_fusion
  227.0 1.3 fusion
  228.2 0.3 fusion.32
  228.5 0.2 fusion.33
  228.7 1.4 copy-done.9
  230.1 4.1 %convolution_convert_fusion = bf16[768,2048]{1,0:T(8,128)(2,1)} fusion(f32[768,64]{1,0:T(8,128)S(1)} %get-tuple-element.19, f32[768,640]{1,0:T(8,128)S(1)} %get-tuple-element.17, f32[768,64]{1,0:T(8,128)S(1)} %get-tuple-element.18, f32[768,640]{1,0:T(8,128)S(1)} %get-tuple-element.16, bf16[16,704,128]{2,1,0:T(8,128)(2,1)S(1)} %copy-done.9), kind=kOutput, calls=%fused_computation.5 | convolution fusion | flops 2220490752 | bytes 10354688 | tf_op jit(solution)/shard_map/dot_general | solution.py:472
  234.2 0.0 reduce-scatter.2.cloned.1.call-update
  234.2 34.3 %reduce-scatter.2.cloned.1.call-done = bf16[96,2048]{1,0:T(8,128)(2,1)} async-done(((bf16[768,2048]{1,0:T(8,128)(2,1)}), bf16[96,2048]{1,0:T(8,128)(2,1)}) %reduce-scatter.2.cloned.1.call-update) | async-done | bytes 393232 | tf_op jit(solution)/shard_map/reduce_scatter | solution.py:473
  268.5 1.4 fusion.12
  269.9 1.4 multiply_reduce_fusion
  271.3 2.2 multiply_convert_fusion
  (41 shorter events, 0.4 us)
Async XLA Ops:
  6.5 8.2 %copy-start.4 = (bf16[768,128]{1,0:T(8,128)(2,1)S(1)}, bf16[768,128]{1,0:T(8,128)(2,1)}, u32[]{:S(2)}) copy-start(bf16[768,128]{1,0:T(8,128)(2,1)} %param.19) | copy-start | bytes 589828
  6.5 8.2 %copy-start.3 = (bf16[768,128]{1,0:T(8,128)(2,1)S(1)}, bf16[768,128]{1,0:T(8,128)(2,1)}, u32[]{:S(2)}) copy-start(bf16[768,128]{1,0:T(8,128)(2,1)} %param.20) | copy-start | bytes 589828
  6.5 8.2 %copy-start.6 = (bf16[768,128]{1,0:T(8,128)(2,1)S(1)}, bf16[768,128]{1,0:T(8,128)(2,1)}, u32[]{:S(2)}) copy-start(bf16[768,128]{1,0:T(8,128)(2,1)} %param.23) | copy-start | bytes 589828
  6.5 8.2 %copy-start.5 = (bf16[768,128]{1,0:T(8,128)(2,1)S(1)}, bf16[768,128]{1,0:T(8,128)(2,1)}, u32[]{:S(2)}) copy-start(bf16[768,128]{1,0:T(8,128)(2,1)} %param.24) | copy-start | bytes 589828
  6.5 207.6 %all-gather.2.cloned.1.call-start = ((), (), s32[]{:S(2)}) async-start(), calls=%async_computation.3 | async-start | bytes 3538944 | tf_op jit(solution)/shard_map/all_gather | solution.py:460
  12.5 3.3 %copy-start = (bf16[128,2048]{1,0:T(8,128)(2,1)S(1)}, bf16[128,2048]{1,0:T(8,128)(2,1)}, u32[]{:S(2)}) copy-start(bf16[128,2048]{1,0:T(8,128)(2,1)} %param.28) | copy-start | bytes 1572868
  12.5 3.3 %copy-start.1 = (bf16[128,2048]{1,0:T(8,128)(2,1)S(1)}, bf16[128,2048]{1,0:T(8,128)(2,1)}, u32[]{:S(2)}) copy-start(bf16[128,2048]{1,0:T(8,128)(2,1)} %param.27) | copy-start | bytes 1572868
  144.8 19.0 %copy-start.2 = (bf16[96,2048]{1,0:T(8,128)(2,1)S(1)}, bf16[96,2048]{1,0:T(8,128)(2,1)}, u32[]{:S(2)}) copy-start(bf16[96,2048]{1,0:T(8,128)(2,1)} %param.26) | copy-start | bytes 1179652
  163.8 5.3 %copy-start.7 = (f32[2048]{0:T(1024)S(1)}, f32[2048]{0:T(1024)}, u32[]{:S(2)}) copy-start(f32[2048]{0:T(1024)} %param.29) | copy-start | bytes 24580
  163.8 6.3 %slice-start = ((f32[3,704]{1,0:T(4,128)}), f32[3,640]{1,0:T(4,128)S(1)}, s32[]{:S(2)}) async-start(f32[3,704]{1,0:T(4,128)} %param.32), calls=%async_computation.5 | async-start | bytes 20480 | tf_op jit(solution)/shard_map/slice | solution.py:463
  163.8 6.4 %slice-start.1 = ((f32[3,704]{1,0:T(4,128)}), f32[3,64]{1,0:T(4,128)S(1)}, s32[]{:S(2)}) async-start(f32[3,704]{1,0:T(4,128)} %param.32), calls=%async_computation.6 | async-start | bytes 4096 | tf_op jit(solution)/shard_map/slice | solution.py:463
  163.8 6.4 %slice-start.2 = ((f32[3,704]{1,0:T(4,128)}), f32[3,640]{1,0:T(4,128)S(1)}, s32[]{:S(2)}) async-start(f32[3,704]{1,0:T(4,128)} %param.33), calls=%async_computation.7 | async-start | bytes 20480 | tf_op jit(solution)/shard_map/slice | solution.py:463
  163.8 6.4 %slice-start.3 = ((f32[3,704]{1,0:T(4,128)}), f32[3,64]{1,0:T(4,128)S(1)}, s32[]{:S(2)}) async-start(f32[3,704]{1,0:T(4,128)} %param.33), calls=%async_computation.8 | async-start | bytes 4096 | tf_op jit(solution)/shard_map/slice | solution.py:463
  170.1 98.4 %reduce-scatter.2.cloned.1.call-start = ((), (), s32[]{:S(2)}) async-start(), calls=%async_computation.4 | async-start | bytes 3538944 | tf_op jit(solution)/shard_map/reduce_scatter | solution.py:473
  222.5 4.0 %collective-permute-start = (bf16[2,1408]{1,0:T(2,128)(2,1)S(1)}, bf16[2,1408]{1,0:T(2,128)(2,1)S(1)}, u32[]{:S(2)}, u32[]{:S(2)}) collective-permute-start(bf16[2,1408]{1,0:T(2,128)(2,1)S(1)} %slice.85), channel_id=1, source_target_pairs={{0,8},{8,16},{16,24},{24,32},{32,40},{40,48},{48,56},{56,64},{64,7... | collective-permute-start | bytes 16904 | tf_op jit(solution)/shard_map/ppermute | solution.py:410
  228.2 1.8 copy-start.9
  234.2 37.1 %copy-start.8 = (f32[2048]{0:T(1024)S(1)}, f32[2048]{0:T(1024)}, u32[]{:S(2)}) copy-start(f32[2048]{0:T(1024)} %param.35) | copy-start | bytes 24580
Sparse Core Ops, SparseCore 0:
  170.2 43.8 all-gather.1
  234.3 34.1 reduce-scatter.1

commit v2 on v1

v2 whole, which is shorter than its diff:
```python
import functools

import jax
import jax.numpy as jnp
from jax import lax
from jax.experimental import pallas as pl
from jax.experimental.pallas import tpu as pltpu
from jax.sharding import Mesh
from jax.sharding import PartitionSpec as P

TP = ("tp_0", "tp_1")
SP_TP = ("sp", "tp_0", "tp_1")
LOG2E = 1.4426950408889634
residual_scale = 2.0**0.5
epsilon = 1e-05
MESH = pl.DeviceIdType.MESH
BLK = 768
EXTRA = 32
RQ = 256
F32 = jnp.float32
BF16 = jnp.bfloat16
VMEM_ALL = 67_000_000
OWN = 96
HALF = 1024


def layer_kernel(
    qs_ref,
    ks_ref,
    vs_ref,
    ql_ref,
    kl_ref,
    vl_ref,
    gs_ref,
    gl_ref,
    lanes_ref,
    vw_ref,
    gw_ref,
    down_ref,
    ms_ref,
    ml_ref,
    res_ref,
    mgain_ref,
    fgain_ref,
    taps_ref,
    out_ref,
    kvin,
    qin,
    kvbuf,
    qpair,
    qm,
    gq,
    gk,
    mst,
    lst,
    acc,
    outv,
    upbuf,
    downbuf,
    mixbuf,
    arrived,
    ybuf,
    mixed,
    both,
    halo,
    hid,
    keep,
    sib_out,
    sib_in,
    far_out,
    far_in,
    near_out,
    near_in,
    ssem,
    rsem,
    lsem,
):
    sp = lax.axis_index("sp")
    y = lax.axis_index("tp_0")
    c = lax.axis_index("tp_1")
    z, x = sp // 4, sp % 4
    role = x // 2
    xr, xl = (x + 1) % 4, (x + 3) % 4
    zu, zd = (z + 1) % 4, (z + 3) % 4
    yu, yd = (y + 1) % 4, (y + 3) % 4
    xf, zf, yf = (x + 2) % 4, (z + 2) % 4, (y + 2) % 4
    mate = x + 1 - 2 * (x % 2)
    opp = 3 - x
    diag = opp + 1 - 2 * (opp % 2)
    pair_sp = 15 - sp
    tp = y * 2 + c

    def at(zz, xx):
        return (zz * 4 + xx, y, c)

    right, left = at(z, xr), at(z, xl)
    above, below = at(zu, x), at(zd, x)
    mate_dev, opp_dev = at(z, mate), at(z, opp)
    pair_dev = (pair_sp, y, c)
    y_up, y_down = (sp, yu, c), (sp, yd, c)
    sibling = (sp, y, 1 - c)
    after, before = ((sp + 1) % 16, y, c), ((sp + 15) % 16, y, c)

    barrier = pltpu.get_barrier_semaphore()
    greeted = [right, left, above, below, after, before]
    for d in range(8):
        t = (tp + d) % 8
        if d:
            greeted.append((sp, t // 2, t % 2))
        greeted.append((pair_sp, t // 2, t % 2))
    for dev in greeted:
        pl.semaphore_signal(barrier, inc=1, device_id=dev, device_id_type=MESH)

    lane = lax.broadcasted_iota(jnp.int32, (1, 128), 1)

    for r, (q_ref, k_ref, v_ref, g_ref) in enumerate(
        ((qs_ref, ks_ref, vs_ref, gs_ref), (ql_ref, kl_ref, vl_ref, gl_ref))
    ):
        kvin[r, 0:BLK, 0:128] = k_ref[...]
        kvin[r, 0:BLK, 128:256] = v_ref[...]
        kvin[r, BLK : BLK + EXTRA, :] = lanes_ref[r]
        qin[r, :, 0:128] = q_ref[...]
        packed = jnp.zeros((BLK, 128), F32)
        for h in range(2 - r):
            col = g_ref[:, h : h + 1] * LOG2E
            for i in range(3):
                part = col.astype(BF16).astype(F32)
                packed = jnp.where(lane == 3 * h + i, part, packed)
                col = col - part
        qin[r, :, 128:256] = packed.astype(BF16)

    def up_rows(b, start=0, size=128):
        return upbuf.at[pl.ds(pl.multiple_of(b * 128 + start, 32), size)]

    def down_cols(b):
        return downbuf.at[pl.ds(0, 704), pl.ds(pl.multiple_of(b * 128, 128), 128)]

    def mix_rows(t, start=0, size=256):
        return mixbuf.at[pl.ds(pl.multiple_of(t * 256 + start, 128), size)]

    mine = pl.ds(pl.multiple_of(sp * 128, 128), 128)
    upbuf[mine, 0:640] = vw_ref[:, 0:640]
    upbuf[mine, 640:1280] = gw_ref[:, 0:640]
    upbuf[mine, 1280:1408] = jnp.concatenate([vw_ref[:, 640:704], gw_ref[:, 640:704]], axis=1)
    mixbuf[pl.ds(pl.multiple_of(tp * 256, 256), 128), :] = ms_ref[...]
    mixbuf[pl.ds(pl.multiple_of(tp * 256 + 128, 128), 128), :] = ml_ref[...]
    downbuf[704:768, :] = jnp.zeros((64, 2048), BF16)

    pl.semaphore_wait(barrier, len(greeted))

    sent = []
    counter = [0]
    incoming = {}

    def send(name, ends):
        k = counter[0]
        counter[0] += 1

        def copy(arriving):
            src, dst, dev, landing = ends()
            return pltpu.make_async_remote_copy(
                src_ref=landing if arriving else src,
                dst_ref=landing if arriving else dst,
                send_sem=ssem.at[k],
                recv_sem=rsem.at[k],
                device_id=dev,
                device_id_type=MESH,
            )

        copy(False).start()
        sent.append(copy)
        incoming[name] = copy

    def take(*names):
        for name in names:
            incoming.pop(name)(True).wait_recv()

    cols = {"own": x, "mate": mate, "opp": opp, "diag": diag}

    send("x1m", lambda: (kvin.at[role], kvbuf.at[sp], mate_dev, kvbuf.at[z * 4 + mate]))
    send("x1o", lambda: (kvin.at[1 - role], kvbuf.at[sp], opp_dev, kvbuf.at[z * 4 + opp]))
    send("wz1u_up", lambda: (up_rows(sp), up_rows(sp), above, up_rows(zd * 4 + x)))
    send("wz1d_up", lambda: (up_rows(sp), up_rows(sp), below, up_rows(zu * 4 + x)))
    send("wz1u_dn", lambda: (down_ref, down_cols(sp), above, down_cols(zd * 4 + x)))
    send("wz1d_dn", lambda: (down_ref, down_cols(sp), below, down_cols(zu * 4 + x)))
    send("q", lambda: (qin.at[1 - role], qpair, pair_dev, qpair))
    send("z1u_own", lambda: (kvin.at[role], kvbuf.at[sp], above, kvbuf.at[zd * 4 + x]))
    send("z1d_own", lambda: (kvin.at[role], kvbuf.at[sp], below, kvbuf.at[zu * 4 + x]))
    send("y1u", lambda: (mix_rows(tp), mix_rows(tp), y_up, mix_rows(yd * 2 + c)))
    send("y1d", lambda: (mix_rows(tp), mix_rows(tp), y_down, mix_rows(yu * 2 + c)))
    send("s0", lambda: (mix_rows(tp), mix_rows(tp), sibling, mix_rows(y * 2 + 1 - c)))

    def pass_x(tag, zz, down_src=None):
        b, b_l, b_r = zz * 4 + x, zz * 4 + xl, zz * 4 + xr
        down_src = down_cols(b) if down_src is None else down_src
        send("wx1r_up" + tag, lambda: (up_rows(b), up_rows(b), right, up_rows(b_l)))
        send("wx1l_up" + tag, lambda: (up_rows(b), up_rows(b), left, up_rows(b_r)))
        send("wx1r_dn" + tag, lambda: (down_src, down_cols(b), right, down_cols(b_l)))
        send("wx1l_dn" + tag, lambda: (down_src, down_cols(b), left, down_cols(b_r)))

    pass_x("0", z, down_ref)

    own_kv = pltpu.make_async_copy(kvin.at[role], kvbuf.at[sp], lsem.at[0])
    own_down = pltpu.make_async_copy(down_ref, down_cols(sp), lsem.at[1])
    own_kv.start()
    own_down.start()

    heads = 2 - role
    head_dim = 64 + 64 * role
    scale = jnp.where(role == 0, 0.125 * LOG2E, 128.0**-0.5 * LOG2E).astype(F32)

    def head_lanes(h):
        return (lane >= h * 64) & (lane < h * 64 + head_dim)

    def load_queries(qi, ref):
        packed = ref[:, 128:256].astype(F32)
        for h in range(2):
            ones = jnp.where(head_lanes(h), 1.0, 0.0).astype(BF16)
            qm[qi, h] = ref[:, 0:128] * ones
            picked = (lane >= 3 * h) & (lane < 3 * h + 3)
            total = jnp.sum(jnp.where(picked, packed, 0.0), axis=1, keepdims=True)
            gq[qi, h] = jnp.broadcast_to(total, (BLK, 128))

    load_queries(0, qin.at[role])
    mst[...] = jnp.full(mst.shape, -1e30, F32)
    lst[...] = jnp.zeros(lst.shape, F32)
    acc[...] = jnp.zeros(acc.shape, F32)

    def pass_z(tag):
        col = cols[tag]
        src = kvbuf.at[z * 4 + col]
        send("z1u_" + tag, lambda: (src, src, above, kvbuf.at[zd * 4 + col]))
        send("z1d_" + tag, lambda: (src, src, below, kvbuf.at[zu * 4 + col]))

    take("x1o")
    send("x2", lambda: (kvbuf.at[z * 4 + opp], kvbuf.at[z * 4 + opp], mate_dev, kvbuf.at[z * 4 + diag]))
    take("x1m")
    take("wz1u_up", "wz1d_up", "wz1u_dn", "wz1d_dn")
    b_d, b_u, b_f = zd * 4 + x, zu * 4 + x, zf * 4 + x
    send("wz2u", lambda: (up_rows(b_d, 0, 96), up_rows(b_d, 0, 96), above, up_rows(b_f, 0, 96)))
    send("wz2d", lambda: (up_rows(b_u, 96, 32), up_rows(b_u, 96, 32), below, up_rows(b_f, 96, 32)))
    send("wz2dd", lambda: (down_cols(b_u), down_cols(b_u), below, down_cols(b_f)))
    pass_z("mate")
    pass_z("opp")
    pass_x("d", zd)
    pass_x("u", zu)
    take("x2")
    pass_z("diag")
    take("q")
    load_queries(1, qpair)
    take("wz2u", "wz2d", "wz2dd")
    pass_x("f", zf)
    own_kv.wait()

    def gate_rows(j):
        rows = kvbuf[j, BLK : BLK + EXTRA, :].astype(F32)
        for h in range(2):
            for p in range(3):
                k = h * 9 + p
                g = rows[k : k + 1] + rows[k + 3 : k + 4] + rows[k + 6 : k + 7]
                gk[j * 2 + h, :, p * 256 : (p + 1) * 256] = jnp.broadcast_to(g, (8, 256))

    def tile(qi, j, h, sub, masked):
        rows = pl.ds(sub * RQ, RQ)
        span = (sub + 1) * RQ if masked else BLK
        mask = head_lanes(h)
        s = lax.dot_general(
            qm[qi, h, rows, :],
            kvbuf[j, 0:span, 0:128],
            (((1,), (1,)), ((), ())),
            preferred_element_type=F32,
        )
        gate = gk[j * 2 + h, 0:1, 0:span]
        parts = []
        for g in range(span // 128):
            part = s[:, g * 128 : (g + 1) * 128] * scale - gate[:, g * 128 : (g + 1) * 128]
            if masked and (g + 1) * 128 > sub * RQ:
                col = lax.broadcasted_iota(jnp.int32, (RQ, 128), 1) + (g * 128 - sub * RQ)
                row = lax.broadcasted_iota(jnp.int32, (RQ, 128), 0)
                part = jnp.where(col <= row, part, -1e30)
            parts.append(part)
        peak = functools.reduce(jnp.maximum, parts)
        peak = jnp.max(peak, axis=1, keepdims=True)
        g_here = gq[qi, h, rows, :]
        old = mst[qi, h, rows, :]
        new = jnp.maximum(old, peak + g_here)
        alpha = jnp.exp2(old - new)
        shift = new - g_here
        weights = [jnp.exp2(part - shift) for part in parts]
        mst[qi, h, rows, :] = new
        lst[qi, h, rows, :] = lst[qi, h, rows, :] * alpha + functools.reduce(jnp.add, weights)
        w = jnp.concatenate([a.astype(BF16) for a in weights], axis=1)
        v = kvbuf[j, 0:span, 128:256] * jnp.where(mask, 1.0, 0.0).astype(BF16)
        update = jnp.dot(w, v, preferred_element_type=F32)
        acc[qi, rows, :] = acc[qi, rows, :] * jnp.where(mask, alpha, 1.0) + update

    def attend_row(zz):
        for xx in range(4):
            gate_rows(zz * 4 + xx)

        def for_queries(qi, _):
            qblk = jnp.where(qi == 0, sp, pair_sp)
            full = jnp.clip(qblk - 4 * zz, 0, 4)

            def for_block(jj, _):
                def for_head(h, _):
                    for sub in range(BLK // RQ):
                        tile(qi, zz * 4 + jj, h, sub, False)
                    return 0

                return lax.fori_loop(0, heads, for_head, 0)

            lax.fori_loop(0, full, for_block, 0)

            @pl.when(qblk // 4 == zz)
            def _():
                def for_head(h, _):
                    for sub in range(BLK // RQ):
                        tile(qi, qblk, h, sub, True)
                    return 0

                lax.fori_loop(0, heads, for_head, 0)

            return 0

        lax.fori_loop(0, 2, for_queries, 0)

    def pass_on(tag, name, from_z, dev, landing_z):
        col = cols[tag]

        def ends():
            src = kvbuf.at[from_z * 4 + col]
            return src, src, dev, kvbuf.at[landing_z * 4 + col]

        send(name + tag, ends)

    m_d, m_u, m_f = yd * 2 + c, yu * 2 + c, yf * 2 + c
    s_d, s_u, s_f = yd * 2 + 1 - c, yu * 2 + 1 - c, yf * 2 + 1 - c

    def pass_x2(tag, zz, name, col, dev):

        def ends(part):
            src = part(zz * 4 + col)
            return src, src, dev, part(zz * 4 + xf)

        send(name + "_up" + tag, lambda: ends(up_rows))
        send(name + "_dn" + tag, lambda: ends(down_cols))

    def one_row(step, _):
        offset = jnp.where(step == 1, 3, jnp.where(step == 2, 1, jnp.where(step == 3, 2, 0)))
        attend_row((z + offset) % 4)

        @pl.when(step == 0)
        def _():
            take("z1u_own", "z1d_own", "z1u_mate", "z1d_mate")
            pass_on("own", "z2u_", zd, above, zf)
            pass_on("mate", "z2u_", zd, above, zf)
            take("z1u_opp", "z1d_opp", "z1u_diag", "z1d_diag")
            pass_on("opp", "z2d_", zu, below, zf)
            pass_on("diag", "z2d_", zu, below, zf)
            take("y1u", "y1d")
            send("y2u", lambda: (mix_rows(m_d, 0, 128), mix_rows(m_d, 0, 128), y_up, mix_rows(m_f, 0, 128)))
            send("y2d", lambda: (mix_rows(m_u, 128, 128), mix_rows(m_u, 128, 128), y_down, mix_rows(m_f, 128, 128)))
            send("s1", lambda: (mix_rows(m_d), mix_rows(m_d), sibling, mix_rows(s_d)))
            send("s2", lambda: (mix_rows(m_u), mix_rows(m_u), sibling, mix_rows(s_u)))

        @pl.when(step == 2)
        def _():
            for tag in ("0", "d", "u", "f"):
                take("wx1r_up" + tag, "wx1r_dn" + tag, "wx1l_up" + tag, "wx1l_dn" + tag)
            pass_x2("0", z, "wx2r", xl, right)
            pass_x2("u", zu, "wx2l", xr, left)
            take("y2u", "y2d")
            send("s3", lambda: (mix_rows(m_f), mix_rows(m_f), sibling, mix_rows(s_f)))
            take("z2u_own", "z2u_mate", "z2d_opp", "z2d_diag")

        return 0

    lax.fori_loop(0, 4, one_row, 0)

    keep0 = head_lanes(0)
    for qi in (1, 0):
        l0 = jnp.sum(lst[qi, 0], axis=1, keepdims=True)
        l1 = jnp.sum(lst[qi, 1], axis=1, keepdims=True)
        outv[qi] = (acc[qi] / jnp.where(keep0, l0, l1)).astype(BF16)

    def own_rows(t):
        return pl.ds(pl.multiple_of(t * OWN, 32), OWN)

    slot = tp * 2 + role

    def send_out(d):
        t, s = (tp + d) % 8, (tp + 8 - d) % 8
        dst = (t // 2, t % 2)
        send(
            "p%d" % d,
            lambda: (outv.at[1, own_rows(t)], arrived.at[slot], (pair_sp, *dst), arrived.at[s * 2 + 1 - role]),
        )
        if d:
            send(
                "a%d" % d,
                lambda: (outv.at[0, own_rows(t)], arrived.at[slot], (sp, *dst), arrived.at[s * 2 + role]),
            )

    for d in range(8):
        send_out(d)
    pass_x2("d", zd, "wx2r", xl, right)
    pass_x2("f", zf, "wx2l", xr, left)
    arrived[slot] = outv[0, own_rows(tp), :]
    take("s0", "s1", "s2", "s3")
    for d in range(8):
        take("p%d" % d)
        if d:
            take("a%d" % d)

    def project(i, _):
        col = pl.ds(pl.multiple_of(i * 256, 256), 256)
        lhs = jnp.concatenate([arrived[s] for s in range(16)], axis=1)
        part = jnp.dot(lhs, mixbuf[:, col], preferred_element_type=F32)
        ybuf[:, col] = residual_scale * res_ref[:, col].astype(F32) + part
        return 0

    lax.fori_loop(0, 8, project, 0)

    def norm(values, gain):
        center = jnp.mean(values, axis=1, keepdims=True)
        off = values - center
        spread = jnp.mean(jnp.square(off), axis=1, keepdims=True)
        return off * lax.rsqrt(spread + epsilon) * gain

    def first_norm(i, _):
        r = pl.ds(pl.multiple_of(i * 16, 16), 16)
        t = pl.ds(pl.multiple_of(tp * OWN + i * 16, 16), 16)
        mixed[t, :] = norm(ybuf[r, :], mgain_ref[...]).astype(BF16)
        return 0

    lax.fori_loop(0, OWN // 16, first_norm, 0)

    def rows_of(t, start=0, size=OWN):
        return mixed.at[pl.ds(pl.multiple_of(t * OWN + start, 16), size)]

    send("gu", lambda: (rows_of(tp), rows_of(tp), y_up, rows_of(m_d)))
    send("gd", lambda: (rows_of(tp), rows_of(tp), y_down, rows_of(m_u)))
    send("gs", lambda: (rows_of(tp), rows_of(tp), sibling, rows_of(y * 2 + 1 - c)))
    own_down.wait()
    for tag in ("0", "d"):
        take("wx2r_up" + tag, "wx2r_dn" + tag)
    for tag in ("u", "f"):
        take("wx2l_up" + tag, "wx2l_dn" + tag)

    def up_group(yy):
        rows = pl.ds(pl.multiple_of(yy * 192, 64), 192)
        into = pl.ds(pl.multiple_of(yy * 192 + 16, 16), 192)

        def some(i, _):
            col = pl.ds(pl.multiple_of(i * 256, 256), 256)
            part = jnp.dot(mixed[rows, :], upbuf[:, col], preferred_element_type=F32)
            both[into, col] = part.astype(BF16)
            return 0

        lax.fori_loop(0, 5, some, 0)
        part = jnp.dot(mixed[rows, :], upbuf[:, 1280:1408], preferred_element_type=F32)
        both[into, 1280:1408] = part.astype(BF16)

    def up_step(step, _):
        @pl.when(step == 0)
        def _():
            take("gs")

        @pl.when(step == 1)
        def _():
            take("gu", "gd")
            send("g2u", lambda: (rows_of(m_d, 0, 48), rows_of(m_d, 0, 48), y_up, rows_of(m_f, 0, 48)))
            send("g2d", lambda: (rows_of(m_u, 48, 48), rows_of(m_u, 48, 48), y_down, rows_of(m_f, 48, 48)))
            send("gs1", lambda: (rows_of(m_d), rows_of(m_d), sibling, rows_of(s_d)))
            send("gs2", lambda: (rows_of(m_u), rows_of(m_u), sibling, rows_of(s_u)))
            take("gs1")

        @pl.when(step == 2)
        def _():
            take("gs2", "g2u", "g2d")
            send("gs3", lambda: (rows_of(m_f), rows_of(m_f), sibling, rows_of(s_f)))

        @pl.when(step == 3)
        def _():
            take("gs3")

        offset = jnp.where(step == 1, 3, jnp.where(step == 2, 1, jnp.where(step == 3, 2, 0)))
        up_group((y + offset) % 4)
        return 0

    lax.fori_loop(0, 4, up_step, 0)
    send("halo", lambda: (both.at[pl.ds(BLK, 16)], halo, after, halo))

    def filtered(a, lanes_):
        taps = taps_ref[:, lanes_]
        n = a.shape[0] - 16
        return (
            taps[0:1] * a[14 : 14 + n]
            + taps[1:2] * a[15 : 15 + n]
            + taps[2:3] * a[16 : 16 + n]
        )

    def hidden_rows(i):
        src = pl.ds(pl.multiple_of(i * OWN, 32), OWN + 16)
        dst = pl.ds(pl.multiple_of(i * OWN, 32), OWN)
        for g in range(6):
            if g < 5:
                at_v, at_g = slice(g * 128, (g + 1) * 128), slice(640 + g * 128, 768 + g * 128)
                fv = filtered(both[src, at_v].astype(F32), at_v)
                fg = filtered(both[src, at_g].astype(F32), at_g)
            else:
                last = slice(1280, 1408)
                fv = filtered(both[src, last].astype(F32), last)
                fg = pltpu.roll(fv, 64, 1)
            value = fg / (1.0 + jnp.exp(-fg)) * fv
            if g == 5:
                value = jnp.where(lane < 64, value, 0.0)
            hid[dst, g * 128 : (g + 1) * 128] = value.astype(BF16)

    def hidden_step(i, _):
        @pl.when(i == 7)
        def _():
            take("halo")
            both[0:16, :] = jnp.where(sp == 0, 0.0, halo[...].astype(F32)).astype(BF16)

        hidden_rows((i + 1) % 8)
        return 0

    lax.fori_loop(0, 8, hidden_step, 0)

    def down_group(g, yy):
        mine = hid[pl.ds(pl.multiple_of(yy * 192 + c * OWN, 32), OWN), :]
        other = hid[pl.ds(pl.multiple_of(yy * 192 + (1 - c) * OWN, 32), OWN), :]
        lhs = jnp.concatenate([mine, other], axis=0)

        def some(i, _):
            col = pl.ds(pl.multiple_of(i * 256, 256), 256)
            part = jnp.dot(lhs, downbuf[:, col], preferred_element_type=F32)
            keep[g, :, col] = part[:OWN]
            sib_out[g, :, col] = part[OWN:].astype(BF16)
            return 0

        lax.fori_loop(0, 8, some, 0)

    def send_sib(g):
        send("r%d" % g, lambda: (sib_out.at[g], sib_in.at[g], sibling, sib_in.at[g]))

    def pair_sum(g, lo, hi):
        return keep[g, :, lo:hi] + sib_in[g, :, lo:hi].astype(F32)

    down_group(0, yf)
    send_sib(0)
    down_group(1, yd)
    send_sib(1)
    take("r0")
    far_out[0] = pair_sum(0, 0, HALF).astype(BF16)
    far_out[1] = pair_sum(0, HALF, 2 * HALF).astype(BF16)
    send("fu", lambda: (far_out.at[0], far_in.at[0], y_up, far_in.at[0]))
    send("fd", lambda: (far_out.at[1], far_in.at[1], y_down, far_in.at[1]))
    down_group(2, yu)
    send_sib(2)
    down_group(3, y)
    send_sib(3)
    take("r1", "r2")
    near_out[0, :, HALF:] = pair_sum(2, HALF, 2 * HALF).astype(BF16)
    near_out[1, :, :HALF] = pair_sum(1, 0, HALF).astype(BF16)
    take("fu")
    near_out[0, :, :HALF] = (pair_sum(2, 0, HALF) + far_in[0].astype(F32)).astype(BF16)
    send("nu", lambda: (near_out.at[0], near_in.at[0], y_up, near_in.at[0]))
    take("fd")
    near_out[1, :, HALF:] = (pair_sum(1, HALF, 2 * HALF) + far_in[1].astype(F32)).astype(BF16)
    send("nd", lambda: (near_out.at[1], near_in.at[1], y_down, near_in.at[1]))
    take("r3", "nu", "nd")

    def last_norm(i, _):
        r = pl.ds(pl.multiple_of(i * 16, 16), 16)
        t = pl.ds(pl.multiple_of(tp * OWN + i * 16, 16), 16)
        ffn = (
            keep[3, r, :]
            + sib_in[3, r, :].astype(F32)
            + near_in[0, r, :].astype(F32)
            + near_in[1, r, :].astype(F32)
        )
        whole = residual_scale * mixed[t, :].astype(F32) + ffn
        out_ref[r, :] = norm(whole, fgain_ref[...]).astype(BF16)
        return 0

    lax.fori_loop(0, OWN // 16, last_norm, 0)
    for copy in sent:
        copy(False).wait_send()


def whole_layer(*operands):
    vmem = pl.BlockSpec(memory_space=pltpu.VMEM)
    return pl.pallas_call(
        layer_kernel,
        out_shape=jax.ShapeDtypeStruct((OWN, 2048), BF16),
        in_specs=[vmem] * len(operands),
        out_specs=vmem,
        scratch_shapes=[
            pltpu.VMEM((2, BLK + EXTRA, 256), BF16),
            pltpu.VMEM((2, BLK, 256), BF16),
            pltpu.VMEM((16, BLK + EXTRA, 256), BF16),
            pltpu.VMEM((BLK, 256), BF16),
            pltpu.VMEM((2, 2, BLK, 128), BF16),
            pltpu.VMEM((2, 2, BLK, 128), F32),
            pltpu.VMEM((32, 8, BLK), F32),
            pltpu.VMEM((2, 2, BLK, 128), F32),
            pltpu.VMEM((2, 2, BLK, 128), F32),
            pltpu.VMEM((2, BLK, 128), F32),
            pltpu.VMEM((2, BLK, 128), BF16),
            pltpu.VMEM((2048, 1408), BF16),
            pltpu.VMEM((768, 2048), BF16),
            pltpu.VMEM((2048, 2048), BF16),
            pltpu.VMEM((16, OWN, 128), BF16),
            pltpu.VMEM((OWN, 2048), F32),
            pltpu.VMEM((BLK, 2048), BF16),
            pltpu.VMEM((BLK + 16, 1408), BF16),
            pltpu.VMEM((16, 1408), BF16),
            pltpu.VMEM((BLK, 768), BF16),
            pltpu.VMEM((4, OWN, 2048), F32),
            pltpu.VMEM((4, OWN, 2048), BF16),
            pltpu.VMEM((4, OWN, 2048), BF16),
            pltpu.VMEM((2, OWN, HALF), BF16),
            pltpu.VMEM((2, OWN, HALF), BF16),
            pltpu.VMEM((2, OWN, 2048), BF16),
            pltpu.VMEM((2, OWN, 2048), BF16),
            pltpu.SemaphoreType.DMA((112,)),
            pltpu.SemaphoreType.DMA((112,)),
            pltpu.SemaphoreType.DMA((2,)),
        ],
        compiler_params=pltpu.CompilerParams(
            collective_id=1, has_side_effects=True, vmem_limit_bytes=VMEM_ALL
        ),
        cost_estimate=pl.CostEstimate(flops=20_000_000_000, bytes_accessed=40_000_000, transcendentals=0),
    )(*operands)


def gate_lanes(gates):
    scaled = gates.T * LOG2E
    high = lax.reduce_precision(scaled, 8, 7)
    middle = lax.reduce_precision(scaled - high, 8, 7)
    low = lax.reduce_precision(scaled - high - middle, 8, 7)
    parts = jnp.stack([high, middle, low], axis=1).astype(BF16)
    rows = parts.reshape(gates.shape[1] * 9, 256)
    return jnp.pad(rows, ((0, EXTRA - rows.shape[0]), (0, 0)))


def per_device(
    query_small,
    key_small,
    value_small,
    gates_small,
    query_large,
    key_large,
    value_large,
    gates_large,
    residual,
    mixer_small,
    mixer_large,
    mix_gain,
    value_weight,
    gate_weight,
    value_taps,
    gate_taps,
    down_weight,
    final_gain,
):
    lanes = jnp.stack([gate_lanes(gates_small), gate_lanes(gates_large)])
    taps = jnp.concatenate(
        [value_taps[:, :640], gate_taps[:, :640], value_taps[:, 640:], gate_taps[:, 640:]], axis=1
    )
    return whole_layer(
        query_small,
        key_small,
        value_small,
        query_large,
        key_large,
        value_large,
        gates_small,
        gates_large,
        lanes,
        value_weight,
        gate_weight,
        down_weight,
        mixer_small,
        mixer_large,
        residual,
        mix_gain[None],
        final_gain[None],
        taps,
    )


def solution(mesh):
    split = Mesh(mesh.devices.reshape(mesh.shape["sp"], 4, 2), ("sp", "tp_0", "tp_1"))
    placed = (
        P("sp", TP),
        P("sp", TP),
        P("sp", TP),
        P("sp", TP),
        P("sp", TP),
        P("sp", TP),
        P("sp", TP),
        P("sp", TP),
        P(SP_TP, None),
        P(TP, None),
        P(TP, None),
        P(),
        P("sp", TP),
        P("sp", TP),
        P(None, TP),
        P(None, TP),
        P(TP, "sp"),
        P(),
    )
    return jax.shard_map(
        per_device, mesh=split, in_specs=placed, out_specs=P(SP_TP, None), check_vma=False
    )
```

time: 283 us -> 195 us (0.69)
  the two profiles are of different devices: /device:TPU:1 before, /device:TPU:40 now
where the time goes in v2:
time: 195 us
  Pallas kernels  184 us (94%)
  local copies, waits for them, and re-layouts  8.97 us (5%)
    pallas_call x1, Pallas kernels, whole_layer(): pl.pallas_call(layer_kernel, out_shape=jax.ShapeDtypeStruct((OWN, 2048),...  184 us
    unnamed x13, local copies, waits for them, and re-layouts  5.42 us

profile of v2, /device:TPU:40, one launch (start us, length us, event | category | flops | bytes accessed | tf_op | source)
XLA Modules:
  0.0 194.6 jit_solution(11037416548557927393)
XLA Ops:
  0.0 0.0 copy-start.2
  0.0 0.0 copy-start
  0.0 0.7 slice.14
  0.7 0.7 slice.15
  1.4 0.0 copy-done.2
  1.5 0.7 reduce-precision_convert_fusion.3
  2.2 0.7 slice.12
  2.9 0.7 slice.13
  3.6 0.7 concatenate.6.taps_ref
  4.3 0.6 pad_maximum_fusion.lanes_ref
  4.9 0.0 copy-done
  4.9 0.0 copy-start.1
  4.9 0.8 copy.27.vw_ref
  5.8 0.1 copy-done.1
  5.9 0.8 copy.28.gw_ref
  6.7 0.0 copy-start.3
  6.7 0.9 copy.25.gs_ref
  7.6 0.0 copy-done.3
  7.6 0.9 copy.26.gl_ref
  8.6 184.2 %shard_map.172 = bf16[96,2048]{1,0:T(8,128)(2,1)} custom-call(bf16[768,128]{1,0:T(8,128)(2,1)} %qs_ref.1, bf16[768,128]{1,0:T(8,128)(2,1)} %ks_ref.1, bf16[768,128]{1,0:T(8,128)(2,1)} %vs_ref.1, bf16[768,128]{1,0:T(8,128)(2,1)} %ql_ref.1, bf16[768,128]{1,0:T(8,128)(2,1)} %kl_ref.1, bf16[768,128]{1,0:T(8,128)(2,1)} %vl_ref.1, f32[768,2]{1,0:T(8,128)} %copy.25.gs_ref, ...), custom_call_target="tpu_custom_call" | custom-call | flops 20000000000 | bytes 40000000 | tf_op jit(solution)/shard_map/pallas_call | solution.py:596
  192.8 1.8 copy.30
  (7 shorter events, 0.1 us)
Async XLA Ops:
  0.0 1.4 copy-start.2
  0.0 4.9 %copy-start = (bf16[128,704]{0,1:T(8,128)(2,1)S(1)}, bf16[128,704]{0,1:T(8,128)(2,1)}, u32[]{:S(2)}) copy-start(bf16[128,704]{0,1:T(8,128)(2,1)} %param.30) | copy-start | bytes 540676
  4.9 0.9 copy-start.1
  6.7 0.9 copy-start.3

commit v3 on v2

--- a/solution.py
+++ b/solution.py
@@ -16,7 +16,9 @@
 MESH = pl.DeviceIdType.MESH
 BLK = 768
 EXTRA = 32
-RQ = 256
+WROWS = 2112
+WHALF = 1056
+RQ = 384
 F32 = jnp.float32
 BF16 = jnp.bfloat16
 VMEM_ALL = 67_000_000
@@ -33,7 +35,6 @@
     vl_ref,
     gs_ref,
     gl_ref,
-    lanes_ref,
     vw_ref,
     gw_ref,
     down_ref,
@@ -42,27 +43,32 @@
     res_ref,
     mgain_ref,
     fgain_ref,
-    taps_ref,
+    vtaps_ref,
+    gtaps_ref,
     out_ref,
     kvin,
     qin,
     kvbuf,
     qpair,
+    qgate,
     qm,
     gq,
     gk,
     mst,
     lst,
     acc,
+    sbuf,
+    pbuf,
+    abuf,
     outv,
-    upbuf,
-    downbuf,
+    wbuf,
     mixbuf,
     arrived,
     ybuf,
     mixed,
     both,
     halo,
+    taps,
     hid,
     keep,
     sib_out,
@@ -118,33 +124,32 @@
     ):
         kvin[r, 0:BLK, 0:128] = k_ref[...]
         kvin[r, 0:BLK, 128:256] = v_ref[...]
-        kvin[r, BLK : BLK + EXTRA, :] = lanes_ref[r]
-        qin[r, :, 0:128] = q_ref[...]
-        packed = jnp.zeros((BLK, 128), F32)
+        qin[r] = q_ref[...]
+        pieces = []
         for h in range(2 - r):
-            col = g_ref[:, h : h + 1] * LOG2E
+            left_over = g_ref[h : h + 1, :] * LOG2E
             for i in range(3):
-                part = col.astype(BF16).astype(F32)
-                packed = jnp.where(lane == 3 * h + i, part, packed)
-                col = col - part
-        qin[r, :, 128:256] = packed.astype(BF16)
-
-    def up_rows(b, start=0, size=128):
-        return upbuf.at[pl.ds(pl.multiple_of(b * 128 + start, 32), size)]
-
-    def down_cols(b):
-        return downbuf.at[pl.ds(0, 704), pl.ds(pl.multiple_of(b * 128, 128), 128)]
+                part = left_over.astype(BF16).astype(F32)
+                left_over = left_over - part
+                pieces += [part[:, p * 256 : (p + 1) * 256] for p in range(3)]
+        pieces.append(jnp.zeros((EXTRA - len(pieces), 256), F32))
+        kvin[r, BLK : BLK + EXTRA, :] = jnp.concatenate(pieces, axis=0).astype(BF16)
 
     def mix_rows(t, start=0, size=256):
         return mixbuf.at[pl.ds(pl.multiple_of(t * 256 + start, 128), size)]
 
-    mine = pl.ds(pl.multiple_of(sp * 128, 128), 128)
-    upbuf[mine, 0:640] = vw_ref[:, 0:640]
-    upbuf[mine, 640:1280] = gw_ref[:, 0:640]
-    upbuf[mine, 1280:1408] = jnp.concatenate([vw_ref[:, 640:704], gw_ref[:, 640:704]], axis=1)
+    def weights(b, start=0, size=WROWS):
+        return wbuf.at[b, pl.ds(start, size)]
+
+    wbuf[sp, 0:640, :] = vw_ref[0:640, :]
+    wbuf[sp, 640:1280, :] = gw_ref[0:640, :]
+    wbuf[sp, 1280:1344, :] = vw_ref[640:704, :]
+    wbuf[sp, 1344:1408, :] = gw_ref[640:704, :]
+    wbuf[sp, 1408:WROWS, :] = down_ref[...]
+    for b in range(16):
+        wbuf[b, WROWS : WROWS + 64, :] = jnp.zeros((64, 128), BF16)
     mixbuf[pl.ds(pl.multiple_of(tp * 256, 256), 128), :] = ms_ref[...]
     mixbuf[pl.ds(pl.multiple_of(tp * 256 + 128, 128), 128), :] = ml_ref[...]
-    downbuf[704:768, :] = jnp.zeros((64, 2048), BF16)
 
     pl.semaphore_wait(barrier, len(greeted))
 
@@ -179,31 +184,25 @@
 
     send("x1m", lambda: (kvin.at[role], kvbuf.at[sp], mate_dev, kvbuf.at[z * 4 + mate]))
     send("x1o", lambda: (kvin.at[1 - role], kvbuf.at[sp], opp_dev, kvbuf.at[z * 4 + opp]))
-    send("wz1u_up", lambda: (up_rows(sp), up_rows(sp), above, up_rows(zd * 4 + x)))
-    send("wz1d_up", lambda: (up_rows(sp), up_rows(sp), below, up_rows(zu * 4 + x)))
-    send("wz1u_dn", lambda: (down_ref, down_cols(sp), above, down_cols(zd * 4 + x)))
-    send("wz1d_dn", lambda: (down_ref, down_cols(sp), below, down_cols(zu * 4 + x)))
-    send("q", lambda: (qin.at[1 - role], qpair, pair_dev, qpair))
     send("z1u_own", lambda: (kvin.at[role], kvbuf.at[sp], above, kvbuf.at[zd * 4 + x]))
     send("z1d_own", lambda: (kvin.at[role], kvbuf.at[sp], below, kvbuf.at[zu * 4 + x]))
+    gate_part = pl.ds(BLK, EXTRA)
+    send("qg", lambda: (kvin.at[1 - role, gate_part], qgate, pair_dev, qgate))
+    send("q", lambda: (qin.at[1 - role], qpair, pair_dev, qpair))
     send("y1u", lambda: (mix_rows(tp), mix_rows(tp), y_up, mix_rows(yd * 2 + c)))
     send("y1d", lambda: (mix_rows(tp), mix_rows(tp), y_down, mix_rows(yu * 2 + c)))
     send("s0", lambda: (mix_rows(tp), mix_rows(tp), sibling, mix_rows(y * 2 + 1 - c)))
 
-    def pass_x(tag, zz, down_src=None):
-        b, b_l, b_r = zz * 4 + x, zz * 4 + xl, zz * 4 + xr
-        down_src = down_cols(b) if down_src is None else down_src
-        send("wx1r_up" + tag, lambda: (up_rows(b), up_rows(b), right, up_rows(b_l)))
-        send("wx1l_up" + tag, lambda: (up_rows(b), up_rows(b), left, up_rows(b_r)))
-        send("wx1r_dn" + tag, lambda: (down_src, down_cols(b), right, down_cols(b_l)))
-        send("wx1l_dn" + tag, lambda: (down_src, down_cols(b), left, down_cols(b_r)))
-
-    pass_x("0", z, down_ref)
+    def pass_x(tag, zz):
+        def ends(dev, col):
+            mine = weights(zz * 4 + x)
+            return mine, mine, dev, weights(zz * 4 + col)
+
+        send("wx1r" + tag, lambda: ends(right, xl))
+        send("wx1l" + tag, lambda: ends(left, xr))
 
     own_kv = pltpu.make_async_copy(kvin.at[role], kvbuf.at[sp], lsem.at[0])
-    own_down = pltpu.make_async_copy(down_ref, down_cols(sp), lsem.at[1])
     own_kv.start()
-    own_down.start()
 
     heads = 2 - role
     head_dim = 64 + 64 * role
@@ -212,16 +211,25 @@
     def head_lanes(h):
         return (lane >= h * 64) & (lane < h * 64 + head_dim)
 
-    def load_queries(qi, ref):
-        packed = ref[:, 128:256].astype(F32)
+    def gate_row(rows, h, g):
+        k, at_ = h * 9 + g // 2, slice((g % 2) * 128, (g % 2) * 128 + 128)
+        return rows[k : k + 1, at_] + rows[k + 3 : k + 4, at_] + rows[k + 6 : k + 7, at_]
+
+    same = lax.broadcasted_iota(jnp.int32, (128, 128), 0) == lax.broadcasted_iota(
+        jnp.int32, (128, 128), 1
+    )
+
+    def load_queries(qi, queries, gate_block):
+        rows = gate_block.astype(F32)
         for h in range(2):
             ones = jnp.where(head_lanes(h), 1.0, 0.0).astype(BF16)
-            qm[qi, h] = ref[:, 0:128] * ones
-            picked = (lane >= 3 * h) & (lane < 3 * h + 3)
-            total = jnp.sum(jnp.where(picked, packed, 0.0), axis=1, keepdims=True)
-            gq[qi, h] = jnp.broadcast_to(total, (BLK, 128))
-
-    load_queries(0, qin.at[role])
+            qm[qi, h] = queries * ones
+            for g in range(BLK // 128):
+                line = jnp.broadcast_to(gate_row(rows, h, g), (128, 128))
+                column = jnp.sum(jnp.where(same, line, 0.0), axis=1, keepdims=True)
+                gq[qi, h, g * 128 : (g + 1) * 128, :] = jnp.broadcast_to(column, (128, 128))
+
+    load_queries(0, qin[role], kvin[role, BLK : BLK + EXTRA, :])
     mst[...] = jnp.full(mst.shape, -1e30, F32)
     lst[...] = jnp.zeros(lst.shape, F32)
     acc[...] = jnp.zeros(acc.shape, F32)
@@ -235,41 +243,48 @@
     take("x1o")
     send("x2", lambda: (kvbuf.at[z * 4 + opp], kvbuf.at[z * 4 + opp], mate_dev, kvbuf.at[z * 4 + diag]))
     take("x1m")
-    take("wz1u_up", "wz1d_up", "wz1u_dn", "wz1d_dn")
+    send("wz1u", lambda: (weights(sp), weights(sp), above, weights(zd * 4 + x)))
+    send("wz1d", lambda: (weights(sp), weights(sp), below, weights(zu * 4 + x)))
+    pass_x("0", z)
+    take("q", "qg")
+    load_queries(1, qpair[...], qgate[...])
+    own_kv.wait()
+    take("wz1u", "wz1d")
     b_d, b_u, b_f = zd * 4 + x, zu * 4 + x, zf * 4 + x
-    send("wz2u", lambda: (up_rows(b_d, 0, 96), up_rows(b_d, 0, 96), above, up_rows(b_f, 0, 96)))
-    send("wz2d", lambda: (up_rows(b_u, 96, 32), up_rows(b_u, 96, 32), below, up_rows(b_f, 96, 32)))
-    send("wz2dd", lambda: (down_cols(b_u), down_cols(b_u), below, down_cols(b_f)))
+    send(
+        "wz2u",
+        lambda: (weights(b_d, 0, WHALF), weights(b_d, 0, WHALF), above, weights(b_f, 0, WHALF)),
+    )
+    send(
+        "wz2d",
+        lambda: (weights(b_u, WHALF, WHALF), weights(b_u, WHALF, WHALF), below, weights(b_f, WHALF, WHALF)),
+    )
     pass_z("mate")
     pass_z("opp")
     pass_x("d", zd)
     pass_x("u", zu)
     take("x2")
     pass_z("diag")
-    take("q")
-    load_queries(1, qpair)
-    take("wz2u", "wz2d", "wz2dd")
-    pass_x("f", zf)
-    own_kv.wait()
-
     def gate_rows(j):
         rows = kvbuf[j, BLK : BLK + EXTRA, :].astype(F32)
         for h in range(2):
-            for p in range(3):
-                k = h * 9 + p
-                g = rows[k : k + 1] + rows[k + 3 : k + 4] + rows[k + 6 : k + 7]
-                gk[j * 2 + h, :, p * 256 : (p + 1) * 256] = jnp.broadcast_to(g, (8, 256))
-
-    def tile(qi, j, h, sub, masked):
+            for g in range(BLK // 128):
+                line = jnp.broadcast_to(gate_row(rows, h, g), (8, 128))
+                gk[j * 2 + h, :, g * 128 : (g + 1) * 128] = line
+
+    def scores(qi, j, h, sub, masked):
         rows = pl.ds(sub * RQ, RQ)
         span = (sub + 1) * RQ if masked else BLK
-        mask = head_lanes(h)
-        s = lax.dot_general(
+        return lax.dot_general(
             qm[qi, h, rows, :],
             kvbuf[j, 0:span, 0:128],
             (((1,), (1,)), ((), ())),
             preferred_element_type=F32,
         )
+
+    def soften(s, qi, j, h, sub, masked):
+        rows = pl.ds(sub * RQ, RQ)
+        span = (sub + 1) * RQ if masked else BLK
         gate = gk[j * 2 + h, 0:1, 0:span]
         parts = []
         for g in range(span // 128):
@@ -289,34 +304,71 @@
         weights = [jnp.exp2(part - shift) for part in parts]
         mst[qi, h, rows, :] = new
         lst[qi, h, rows, :] = lst[qi, h, rows, :] * alpha + functools.reduce(jnp.add, weights)
-        w = jnp.concatenate([a.astype(BF16) for a in weights], axis=1)
+        return jnp.concatenate([a.astype(BF16) for a in weights], axis=1), alpha
+
+    def spread(w, alpha, qi, j, h, sub, masked):
+        rows = pl.ds(sub * RQ, RQ)
+        span = (sub + 1) * RQ if masked else BLK
+        mask = head_lanes(h)
         v = kvbuf[j, 0:span, 128:256] * jnp.where(mask, 1.0, 0.0).astype(BF16)
         update = jnp.dot(w, v, preferred_element_type=F32)
         acc[qi, rows, :] = acc[qi, rows, :] * jnp.where(mask, alpha, 1.0) + update
 
+    def tiles(qi, j, h, masked):
+        count = BLK // RQ
+        s = scores(qi, j, h, 0, masked)
+        held = None
+        for sub in range(count):
+            ahead = scores(qi, j, h, sub + 1, masked) if sub + 1 < count else None
+            w, alpha = soften(s, qi, j, h, sub, masked)
+            spread(w, alpha, qi, j, h, sub, masked)
+            s = ahead
+
     def attend_row(zz):
         for xx in range(4):
             gate_rows(zz * 4 + xx)
 
+        full = [jnp.clip(b - 4 * zz, 0, 4) for b in (sp, pair_sp)]
+        split = full[0] * heads
+        units = split + full[1] * heads
+
+        def place(u):
+            u = jnp.minimum(u, units - 1)
+            qi = jnp.where(u >= split, 1, 0)
+            r = u - qi * split
+            return qi, zz * 4 + r // heads, r % heads
+
+        def finish(u, qi):
+            _, j, h = place(u)
+            spread(pbuf[...], abuf[...], qi, j, h, 1, False)
+
+        def one_unit(u, _):
+            qi, j, h = place(u)
+            before_qi = jnp.where(u > 0, place(jnp.maximum(u - 1, 0))[0], 2)
+            finish(jnp.maximum(u - 1, 0), before_qi)
+            later = scores(qi, j, h, 1, False)
+            w, alpha = soften(sbuf[...], qi, j, h, 0, False)
+            spread(w, alpha, qi, j, h, 0, False)
+            ahead = scores(*place(u + 1), 0, False)
+            w, alpha = soften(later, qi, j, h, 1, False)
+            sbuf[...] = ahead
+            pbuf[...] = w
+            abuf[...] = alpha
+            return 0
+
+        @pl.when(units > 0)
+        def _():
+            sbuf[...] = scores(*place(0), 0, False)
+            lax.fori_loop(0, units, one_unit, 0)
+            finish(units - 1, place(units - 1)[0])
+
         def for_queries(qi, _):
             qblk = jnp.where(qi == 0, sp, pair_sp)
-            full = jnp.clip(qblk - 4 * zz, 0, 4)
-
-            def for_block(jj, _):
-                def for_head(h, _):
-                    for sub in range(BLK // RQ):
-                        tile(qi, zz * 4 + jj, h, sub, False)
-                    return 0
-
-                return lax.fori_loop(0, heads, for_head, 0)
-
-            lax.fori_loop(0, full, for_block, 0)
 
             @pl.when(qblk // 4 == zz)
             def _():
                 def for_head(h, _):
-                    for sub in range(BLK // RQ):
-                        tile(qi, qblk, h, sub, True)
+                    tiles(qi, qblk, h, True)
                     return 0
 
                 lax.fori_loop(0, heads, for_head, 0)
@@ -337,14 +389,12 @@
     m_d, m_u, m_f = yd * 2 + c, yu * 2 + c, yf * 2 + c
     s_d, s_u, s_f = yd * 2 + 1 - c, yu * 2 + 1 - c, yf * 2 + 1 - c
 
-    def pass_x2(tag, zz, name, col, dev):
-
-        def ends(part):
-            src = part(zz * 4 + col)
-            return src, src, dev, part(zz * 4 + xf)
-
-        send(name + "_up" + tag, lambda: ends(up_rows))
-        send(name + "_dn" + tag, lambda: ends(down_cols))
+    def pass_x2(tag, zz, name, col, dev, start=0, size=WROWS):
+        def ends():
+            src = weights(zz * 4 + col, start, size)
+            return src, src, dev, weights(zz * 4 + xf, start, size)
+
+        send(name + tag, ends)
 
     def one_row(step, _):
         offset = jnp.where(step == 1, 3, jnp.where(step == 2, 1, jnp.where(step == 3, 2, 0)))
@@ -352,26 +402,36 @@
 
         @pl.when(step == 0)
         def _():
+            take("y1u", "y1d")
+            send("y2u", lambda: (mix_rows(m_d, 0, 128), mix_rows(m_d, 0, 128), y_up, mix_rows(m_f, 0, 128)))
+            send("y2d", lambda: (mix_rows(m_u, 128, 128), mix_rows(m_u, 128, 128), y_down, mix_rows(m_f, 128, 128)))
+            send("s1", lambda: (mix_rows(m_d), mix_rows(m_d), sibling, mix_rows(s_d)))
+            send("s2", lambda: (mix_rows(m_u), mix_rows(m_u), sibling, mix_rows(s_u)))
             take("z1u_own", "z1d_own", "z1u_mate", "z1d_mate")
             pass_on("own", "z2u_", zd, above, zf)
             pass_on("mate", "z2u_", zd, above, zf)
             take("z1u_opp", "z1d_opp", "z1u_diag", "z1d_diag")
             pass_on("opp", "z2d_", zu, below, zf)
             pass_on("diag", "z2d_", zu, below, zf)
-            take("y1u", "y1d")
-            send("y2u", lambda: (mix_rows(m_d, 0, 128), mix_rows(m_d, 0, 128), y_up, mix_rows(m_f, 0, 128)))
-            send("y2d", lambda: (mix_rows(m_u, 128, 128), mix_rows(m_u, 128, 128), y_down, mix_rows(m_f, 128, 128)))
-            send("s1", lambda: (mix_rows(m_d), mix_rows(m_d), sibling, mix_rows(s_d)))
-            send("s2", lambda: (mix_rows(m_u), mix_rows(m_u), sibling, mix_rows(s_u)))
+            take("wz2u", "wz2d")
+            pass_x("f", zf)
+            take("wx1r0", "wx1l0")
+            pass_x2("0", z, "wx2r", xl, right)
+
+        @pl.when(step == 1)
+        def _():
+            take("wx1rd", "wx1ld", "wx1ru", "wx1lu")
+            pass_x2("d", zd, "wx2l", xr, left)
+            pass_x2("u", zu, "wx2r", xl, right, 0, WHALF)
+            pass_x2("u", zu, "wx2l", xr, left, WHALF, WHALF)
 
         @pl.when(step == 2)
         def _():
-            for tag in ("0", "d", "u", "f"):
-                take("wx1r_up" + tag, "wx1r_dn" + tag, "wx1l_up" + tag, "wx1l_dn" + tag)
-            pass_x2("0", z, "wx2r", xl, right)
-            pass_x2("u", zu, "wx2l", xr, left)
             take("y2u", "y2d")
             send("s3", lambda: (mix_rows(m_f), mix_rows(m_f), sibling, mix_rows(s_f)))
+            take("wx1rf", "wx1lf")
+            pass_x2("f", zf, "wx2r", xl, right, 0, WHALF)
+            pass_x2("f", zf, "wx2l", xr, left, WHALF, WHALF)
             take("z2u_own", "z2u_mate", "z2d_opp", "z2d_diag")
 
         return 0
@@ -404,8 +464,6 @@
 
     for d in range(8):
         send_out(d)
-    pass_x2("d", zd, "wx2r", xl, right)
-    pass_x2("f", zf, "wx2l", xr, left)
     arrived[slot] = outv[0, own_rows(tp), :]
     take("s0", "s1", "s2", "s3")
     for d in range(8):
@@ -442,63 +500,52 @@
     send("gu", lambda: (rows_of(tp), rows_of(tp), y_up, rows_of(m_d)))
     send("gd", lambda: (rows_of(tp), rows_of(tp), y_down, rows_of(m_u)))
     send("gs", lambda: (rows_of(tp), rows_of(tp), sibling, rows_of(y * 2 + 1 - c)))
-    own_down.wait()
-    for tag in ("0", "d"):
-        take("wx2r_up" + tag, "wx2r_dn" + tag)
-    for tag in ("u", "f"):
-        take("wx2l_up" + tag, "wx2l_dn" + tag)
-
-    def up_group(yy):
-        rows = pl.ds(pl.multiple_of(yy * 192, 64), 192)
-        into = pl.ds(pl.multiple_of(yy * 192 + 16, 16), 192)
-
-        def some(i, _):
-            col = pl.ds(pl.multiple_of(i * 256, 256), 256)
-            part = jnp.dot(mixed[rows, :], upbuf[:, col], preferred_element_type=F32)
-            both[into, col] = part.astype(BF16)
+    take("wx2r0", "wx2ld", "wx2ru", "wx2lu", "wx2rf", "wx2lf")
+
+    def up_group(*chips):
+        def some(start, width):
+            cols_ = pl.ds(start, width)
+            rhs = jnp.concatenate([wbuf[b, cols_, :] for b in range(16)], axis=1)
+            lhs = [mixed[pl.ds(pl.multiple_of(yy * 192, 64), 192), :] for yy in chips]
+            part = lax.dot_general(
+                jnp.concatenate(lhs, axis=0), rhs, (((1,), (1,)), ((), ())), preferred_element_type=F32
+            ).astype(BF16)
+            for k, yy in enumerate(chips):
+                into = pl.ds(pl.multiple_of(yy * 192 + 16, 16), 192)
+                both[into, cols_] = part[k * 192 : (k + 1) * 192]
+
+        def chunk(i, _):
+            some(pl.multiple_of(i * 256, 256), 256)
             return 0
 
-        lax.fori_loop(0, 5, some, 0)
-        part = jnp.dot(mixed[rows, :], upbuf[:, 1280:1408], preferred_element_type=F32)
-        both[into, 1280:1408] = part.astype(BF16)
-
-    def up_step(step, _):
-        @pl.when(step == 0)
-        def _():
-            take("gs")
-
-        @pl.when(step == 1)
-        def _():
-            take("gu", "gd")
-            send("g2u", lambda: (rows_of(m_d, 0, 48), rows_of(m_d, 0, 48), y_up, rows_of(m_f, 0, 48)))
-            send("g2d", lambda: (rows_of(m_u, 48, 48), rows_of(m_u, 48, 48), y_down, rows_of(m_f, 48, 48)))
-            send("gs1", lambda: (rows_of(m_d), rows_of(m_d), sibling, rows_of(s_d)))
-            send("gs2", lambda: (rows_of(m_u), rows_of(m_u), sibling, rows_of(s_u)))
-            take("gs1")
-
-        @pl.when(step == 2)
-        def _():
-            take("gs2", "g2u", "g2d")
-            send("gs3", lambda: (rows_of(m_f), rows_of(m_f), sibling, rows_of(s_f)))
-
-        @pl.when(step == 3)
-        def _():
-            take("gs3")
-
-        offset = jnp.where(step == 1, 3, jnp.where(step == 2, 1, jnp.where(step == 3, 2, 0)))
-        up_group((y + offset) % 4)
-        return 0
-
-    lax.fori_loop(0, 4, up_step, 0)
+        lax.fori_loop(0, 5, chunk, 0)
+        some(1280, 128)
+
+    take("gs")
+    up_group(y)
+    take("gu", "gd")
+    send("g2u", lambda: (rows_of(m_d, 0, 48), rows_of(m_d, 0, 48), y_up, rows_of(m_f, 0, 48)))
+    send("g2d", lambda: (rows_of(m_u, 48, 48), rows_of(m_u, 48, 48), y_down, rows_of(m_f, 48, 48)))
+    send("gs1", lambda: (rows_of(m_d), rows_of(m_d), sibling, rows_of(s_d)))
+    send("gs2", lambda: (rows_of(m_u), rows_of(m_u), sibling, rows_of(s_u)))
+    take("gs1", "gs2")
+    up_group(yd, yu)
+    take("g2u", "g2d")
+    send("gs3", lambda: (rows_of(m_f), rows_of(m_f), sibling, rows_of(s_f)))
+    take("gs3")
+    up_group(yf)
     send("halo", lambda: (both.at[pl.ds(BLK, 16)], halo, after, halo))
 
+    taps[0:3, 0:640] = vtaps_ref[:, 0:640]
+    taps[0:3, 640:1280] = gtaps_ref[:, 0:640]
+    taps[0:3, 1280:1408] = jnp.concatenate([vtaps_ref[:, 640:704], gtaps_ref[:, 640:704]], axis=1)
+
     def filtered(a, lanes_):
-        taps = taps_ref[:, lanes_]
         n = a.shape[0] - 16
         return (
-            taps[0:1] * a[14 : 14 + n]
-            + taps[1:2] * a[15 : 15 + n]
-            + taps[2:3] * a[16 : 16 + n]
+            taps[0:1, lanes_] * a[14 : 14 + n]
+            + taps[1:2, lanes_] * a[15 : 15 + n]
+            + taps[2:3, lanes_] * a[16 : 16 + n]
         )
 
     def hidden_rows(i):
@@ -536,7 +583,10 @@
 
         def some(i, _):
             col = pl.ds(pl.multiple_of(i * 256, 256), 256)
-            part = jnp.dot(lhs, downbuf[:, col], preferred_element_type=F32)
+            rhs = jnp.concatenate(
+                [wbuf[2 * i, 1408 : WROWS + 64, :], wbuf[2 * i + 1, 1408 : WROWS + 64, :]], axis=1
+            )
+            part = jnp.dot(lhs, rhs, preferred_element_type=F32)
             keep[g, :, col] = part[:OWN]
             sib_out[g, :, col] = part[OWN:].astype(BF16)
             return 0
@@ -600,24 +650,28 @@
         out_specs=vmem,
         scratch_shapes=[
             pltpu.VMEM((2, BLK + EXTRA, 256), BF16),
-            pltpu.VMEM((2, BLK, 256), BF16),
+            pltpu.VMEM((2, BLK, 128), BF16),
             pltpu.VMEM((16, BLK + EXTRA, 256), BF16),
-            pltpu.VMEM((BLK, 256), BF16),
+            pltpu.VMEM((BLK, 128), BF16),
+            pltpu.VMEM((EXTRA, 256), BF16),
             pltpu.VMEM((2, 2, BLK, 128), BF16),
             pltpu.VMEM((2, 2, BLK, 128), F32),
             pltpu.VMEM((32, 8, BLK), F32),
             pltpu.VMEM((2, 2, BLK, 128), F32),
             pltpu.VMEM((2, 2, BLK, 128), F32),
-            pltpu.VMEM((2, BLK, 128), F32),
+            pltpu.VMEM((3, BLK, 128), F32),
+            pltpu.VMEM((RQ, BLK), F32),
+            pltpu.VMEM((RQ, BLK), BF16),
+            pltpu.VMEM((RQ, 128), F32),
             pltpu.VMEM((2, BLK, 128), BF16),
-            pltpu.VMEM((2048, 1408), BF16),
-            pltpu.VMEM((768, 2048), BF16),
+            pltpu.VMEM((16, WROWS + 64, 128), BF16),
             pltpu.VMEM((2048, 2048), BF16),
             pltpu.VMEM((16, OWN, 128), BF16),
             pltpu.VMEM((OWN, 2048), F32),
             pltpu.VMEM((BLK, 2048), BF16),
             pltpu.VMEM((BLK + 16, 1408), BF16),
             pltpu.VMEM((16, 1408), BF16),
+            pltpu.VMEM((8, 1408), F32),
             pltpu.VMEM((BLK, 768), BF16),
             pltpu.VMEM((4, OWN, 2048), F32),
             pltpu.VMEM((4, OWN, 2048), BF16),
@@ -635,16 +689,6 @@
         ),
         cost_estimate=pl.CostEstimate(flops=20_000_000_000, bytes_accessed=40_000_000, transcendentals=0),
     )(*operands)
-
-
-def gate_lanes(gates):
-    scaled = gates.T * LOG2E
-    high = lax.reduce_precision(scaled, 8, 7)
-    middle = lax.reduce_precision(scaled - high, 8, 7)
-    low = lax.reduce_precision(scaled - high - middle, 8, 7)
-    parts = jnp.stack([high, middle, low], axis=1).astype(BF16)
-    rows = parts.reshape(gates.shape[1] * 9, 256)
-    return jnp.pad(rows, ((0, EXTRA - rows.shape[0]), (0, 0)))
 
 
 def per_device(
@@ -667,10 +711,6 @@
     down_weight,
     final_gain,
 ):
-    lanes = jnp.stack([gate_lanes(gates_small), gate_lanes(gates_large)])
-    taps = jnp.concatenate(
-        [value_taps[:, :640], gate_taps[:, :640], value_taps[:, 640:], gate_taps[:, 640:]], axis=1
-    )
     return whole_layer(
         query_small,
         key_small,
@@ -678,18 +718,18 @@
         query_large,
         key_large,
         value_large,
-        gates_small,
-        gates_large,
-        lanes,
-        value_weight,
-        gate_weight,
+        gates_small.T,
+        gates_large.T,
+        value_weight.T,
+        gate_weight.T,
         down_weight,
         mixer_small,
         mixer_large,
         residual,
         mix_gain[None],
         final_gain[None],
-        taps,
+        value_taps,
+        gate_taps,
     )
 
 

time: 195 us -> 175 us (0.90)
  the two profiles are of different devices: /device:TPU:40 before, /device:TPU:1 now
where the time goes in v3:
time: 175 us; the launch traced here: 172 us
  Pallas kernels  170 us (97%)
  local copies, waits for them, and re-layouts  1.77 us (1%)
    pallas_call x1, Pallas kernels, whole_layer(): pl.pallas_call(layer_kernel, out_shape=jax.ShapeDtypeStruct((OWN, 2048),...  170 us

profile of v3, /device:TPU:1, one launch (start us, length us, event | category | flops | bytes accessed | tf_op | source)
XLA Modules:
  0.0 171.7 jit_solution(14351661606462030600)
XLA Ops:
  0.0 169.9 %shard_map.172 = bf16[96,2048]{1,0:T(8,128)(2,1)} custom-call(bf16[768,128]{1,0:T(8,128)(2,1)} %qs_ref.1, bf16[768,128]{1,0:T(8,128)(2,1)} %ks_ref.1, bf16[768,128]{1,0:T(8,128)(2,1)} %vs_ref.1, bf16[768,128]{1,0:T(8,128)(2,1)} %ql_ref.1, bf16[768,128]{1,0:T(8,128)(2,1)} %kl_ref.1, bf16[768,128]{1,0:T(8,128)(2,1)} %vl_ref.1, f32[2,768]{1,0:T(2,128)} %bitcast.10, ...), custom_call_target="tpu_custom_call" | custom-call | flops 20000000000 | bytes 40000000 | tf_op jit(solution)/shard_map/pallas_call | solution.py:646
  170.0 1.8 %copy.20 = bf16[96,2048]{1,0:T(8,128)(2,1)} copy(bf16[96,2048]{1,0:T(8,128)(2,1)} %shard_map.172) | data formatting | bytes 786432

commit v4 on v3

--- a/solution.py
+++ b/solution.py
@@ -17,13 +17,15 @@
 BLK = 768
 EXTRA = 32
 WROWS = 2112
-WHALF = 1056
+UP = 1408
+DOWN = 704
 RQ = 384
 F32 = jnp.float32
 BF16 = jnp.bfloat16
 VMEM_ALL = 67_000_000
 OWN = 96
 HALF = 1024
+HALO_SEM = 111
 
 
 def layer_kernel(
@@ -58,6 +60,7 @@
     lst,
     acc,
     sbuf,
+    mbuf,
     pbuf,
     abuf,
     outv,
@@ -138,8 +141,11 @@
     def mix_rows(t, start=0, size=256):
         return mixbuf.at[pl.ds(pl.multiple_of(t * 256 + start, 128), size)]
 
-    def weights(b, start=0, size=WROWS):
+    def up_block(b, start=0, size=UP):
         return wbuf.at[b, pl.ds(start, size)]
+
+    def down_blocks(b, count=1, start=0, size=DOWN):
+        return wbuf.at[pl.ds(b, count), pl.ds(UP + start, size)]
 
     wbuf[sp, 0:640, :] = vw_ref[0:640, :]
     wbuf[sp, 640:1280, :] = gw_ref[0:640, :]
@@ -157,7 +163,7 @@
     counter = [0]
     incoming = {}
 
-    def send(name, ends):
+    def send(name, ends, sends=None, receives=None):
         k = counter[0]
         counter[0] += 1
 
@@ -172,20 +178,24 @@
                 device_id_type=MESH,
             )
 
-        copy(False).start()
-        sent.append(copy)
-        incoming[name] = copy
+        def only(condition, act):
+            act() if condition is None else pl.when(condition())(act)
+
+        sent.append(lambda: only(sends, lambda: copy(False).wait_send()))
+        incoming[name] = lambda: only(receives, lambda: copy(True).wait_recv())
+        only(sends, lambda: copy(False).start())
+        return lambda: copy(False).start()
 
     def take(*names):
         for name in names:
-            incoming.pop(name)(True).wait_recv()
+            incoming.pop(name)()
 
     cols = {"own": x, "mate": mate, "opp": opp, "diag": diag}
 
     send("x1m", lambda: (kvin.at[role], kvbuf.at[sp], mate_dev, kvbuf.at[z * 4 + mate]))
     send("x1o", lambda: (kvin.at[1 - role], kvbuf.at[sp], opp_dev, kvbuf.at[z * 4 + opp]))
     send("z1u_own", lambda: (kvin.at[role], kvbuf.at[sp], above, kvbuf.at[zd * 4 + x]))
-    send("z1d_own", lambda: (kvin.at[role], kvbuf.at[sp], below, kvbuf.at[zu * 4 + x]))
+    send("z1d_own", lambda: (kvin.at[role], kvbuf.at[sp], below, kvbuf.at[zu * 4 + x]), lambda: z < 3, lambda: z != 2)
     gate_part = pl.ds(BLK, EXTRA)
     send("qg", lambda: (kvin.at[1 - role, gate_part], qgate, pair_dev, qgate))
     send("q", lambda: (qin.at[1 - role], qpair, pair_dev, qpair))
@@ -195,8 +205,8 @@
 
     def pass_x(tag, zz):
         def ends(dev, col):
-            mine = weights(zz * 4 + x)
-            return mine, mine, dev, weights(zz * 4 + col)
+            mine = up_block(zz * 4 + x)
+            return mine, mine, dev, up_block(zz * 4 + col)
 
         send("wx1r" + tag, lambda: ends(right, xl))
         send("wx1l" + tag, lambda: ends(left, xr))
@@ -238,33 +248,49 @@
         col = cols[tag]
         src = kvbuf.at[z * 4 + col]
         send("z1u_" + tag, lambda: (src, src, above, kvbuf.at[zd * 4 + col]))
-        send("z1d_" + tag, lambda: (src, src, below, kvbuf.at[zu * 4 + col]))
-
+        send("z1d_" + tag, lambda: (src, src, below, kvbuf.at[zu * 4 + col]), lambda: z < 3, lambda: z != 2)
+
+    b_d, b_u, b_f = zd * 4 + x, zu * 4 + x, zf * 4 + x
+    b_l, b_r, b_o = z * 4 + xl, z * 4 + xr, z * 4 + (x + 2) % 4
+    dhalf = DOWN // 2
     take("x1o")
     send("x2", lambda: (kvbuf.at[z * 4 + opp], kvbuf.at[z * 4 + opp], mate_dev, kvbuf.at[z * 4 + diag]))
+    pass_z("opp")
     take("x1m")
-    send("wz1u", lambda: (weights(sp), weights(sp), above, weights(zd * 4 + x)))
-    send("wz1d", lambda: (weights(sp), weights(sp), below, weights(zu * 4 + x)))
+    pass_z("mate")
+    send("wz1u", lambda: (up_block(sp), up_block(sp), above, up_block(b_d)))
+    send("wz1d", lambda: (up_block(sp), up_block(sp), below, up_block(b_u)))
+    send("bx1r", lambda: (down_blocks(sp), down_blocks(sp), right, down_blocks(b_l)))
+    send("bx1l", lambda: (down_blocks(sp), down_blocks(sp), left, down_blocks(b_r)))
     pass_x("0", z)
+    own_kv.wait()
+    take("x2")
+    pass_z("diag")
+    take("z1u_own", "z1d_own")
+    send(
+        "z2u_own",
+        lambda: (kvbuf.at[zd * 4 + x], kvbuf.at[zd * 4 + x], above, kvbuf.at[zf * 4 + x]),
+        lambda: z >= 2,
+        lambda: (z == 0) | (z == 3),
+    )
+    send(
+        "z2x_own",
+        lambda: (kvbuf.at[zu * 4 + x], kvbuf.at[zu * 4 + x], below, kvbuf.at[zf * 4 + x]),
+        lambda: z == 3,
+        lambda: z == 2,
+    )
+    take("bx1r", "bx1l")
+    send(
+        "bx2r",
+        lambda: (down_blocks(b_l, 1, 0, dhalf), down_blocks(b_l, 1, 0, dhalf), right, down_blocks(b_o, 1, 0, dhalf)),
+    )
+    send(
+        "bx2l",
+        lambda: (down_blocks(b_r, 1, dhalf, dhalf), down_blocks(b_r, 1, dhalf, dhalf), left, down_blocks(b_o, 1, dhalf, dhalf)),
+    )
     take("q", "qg")
     load_queries(1, qpair[...], qgate[...])
-    own_kv.wait()
-    take("wz1u", "wz1d")
-    b_d, b_u, b_f = zd * 4 + x, zu * 4 + x, zf * 4 + x
-    send(
-        "wz2u",
-        lambda: (weights(b_d, 0, WHALF), weights(b_d, 0, WHALF), above, weights(b_f, 0, WHALF)),
-    )
-    send(
-        "wz2d",
-        lambda: (weights(b_u, WHALF, WHALF), weights(b_u, WHALF, WHALF), below, weights(b_f, WHALF, WHALF)),
-    )
-    pass_z("mate")
-    pass_z("opp")
-    pass_x("d", zd)
-    pass_x("u", zu)
-    take("x2")
-    pass_z("diag")
+
     def gate_rows(j):
         rows = kvbuf[j, BLK : BLK + EXTRA, :].astype(F32)
         for h in range(2):
@@ -275,36 +301,43 @@
     def scores(qi, j, h, sub, masked):
         rows = pl.ds(sub * RQ, RQ)
         span = (sub + 1) * RQ if masked else BLK
-        return lax.dot_general(
+        raw = lax.dot_general(
             qm[qi, h, rows, :],
             kvbuf[j, 0:span, 0:128],
             (((1,), (1,)), ((), ())),
             preferred_element_type=F32,
         )
-
-    def soften(s, qi, j, h, sub, masked):
-        rows = pl.ds(sub * RQ, RQ)
-        span = (sub + 1) * RQ if masked else BLK
         gate = gk[j * 2 + h, 0:1, 0:span]
         parts = []
         for g in range(span // 128):
-            part = s[:, g * 128 : (g + 1) * 128] * scale - gate[:, g * 128 : (g + 1) * 128]
+            part = raw[:, g * 128 : (g + 1) * 128] * scale - gate[:, g * 128 : (g + 1) * 128]
             if masked and (g + 1) * 128 > sub * RQ:
                 col = lax.broadcasted_iota(jnp.int32, (RQ, 128), 1) + (g * 128 - sub * RQ)
                 row = lax.broadcasted_iota(jnp.int32, (RQ, 128), 0)
                 part = jnp.where(col <= row, part, -1e30)
             parts.append(part)
-        peak = functools.reduce(jnp.maximum, parts)
+        return parts, functools.reduce(jnp.maximum, parts)
+
+    def soften(parts, peak, qi, j, h, sub):
+        rows = pl.ds(sub * RQ, RQ)
         peak = jnp.max(peak, axis=1, keepdims=True)
         g_here = gq[qi, h, rows, :]
         old = mst[qi, h, rows, :]
         new = jnp.maximum(old, peak + g_here)
         alpha = jnp.exp2(old - new)
         shift = new - g_here
-        weights = [jnp.exp2(part - shift) for part in parts]
+        weights_ = [jnp.exp2(part - shift) for part in parts]
         mst[qi, h, rows, :] = new
-        lst[qi, h, rows, :] = lst[qi, h, rows, :] * alpha + functools.reduce(jnp.add, weights)
-        return jnp.concatenate([a.astype(BF16) for a in weights], axis=1), alpha
+        lst[qi, h, rows, :] = lst[qi, h, rows, :] * alpha + functools.reduce(jnp.add, weights_)
+        return jnp.concatenate([a.astype(BF16) for a in weights_], axis=1), alpha
+
+    def hold(parts, peak):
+        for g, part in enumerate(parts):
+            sbuf[:, g * 128 : (g + 1) * 128] = part
+        mbuf[...] = peak
+
+    def held():
+        return [sbuf[:, g * 128 : (g + 1) * 128] for g in range(BLK // 128)], mbuf[...]
 
     def spread(w, alpha, qi, j, h, sub, masked):
         rows = pl.ds(sub * RQ, RQ)
@@ -316,127 +349,142 @@
 
     def tiles(qi, j, h, masked):
         count = BLK // RQ
-        s = scores(qi, j, h, 0, masked)
-        held = None
+        ahead = scores(qi, j, h, 0, masked)
         for sub in range(count):
+            here = ahead
             ahead = scores(qi, j, h, sub + 1, masked) if sub + 1 < count else None
-            w, alpha = soften(s, qi, j, h, sub, masked)
+            w, alpha = soften(*here, qi, j, h, sub)
             spread(w, alpha, qi, j, h, sub, masked)
-            s = ahead
-
-    def attend_row(zz):
-        for xx in range(4):
-            gate_rows(zz * 4 + xx)
-
-        full = [jnp.clip(b - 4 * zz, 0, 4) for b in (sp, pair_sp)]
-        split = full[0] * heads
-        units = split + full[1] * heads
+
+    blocks_of = (sp, pair_sp)
+
+    def attend(step):
+        row = jnp.where(step == 0, z, jnp.where(step == 2, zd, jnp.where(step == 3, zu, zf)))
+        second = step == 1
+        none = 99
+        slots = (
+            jnp.where(second, zd * 4 + x, row * 4 + mate),
+            jnp.where(second, zu * 4 + x, row * 4 + opp),
+            jnp.where(second, none, row * 4 + diag),
+            jnp.where(step == 0, sp, jnp.where(step == 3, zf * 4 + x, none)),
+        )
+        for j in slots:
+            pl.when(j <= jnp.maximum(sp, pair_sp))(functools.partial(gate_rows, j))
+
+        found, count = [], 0
+        for qi in range(2):
+            for j in slots:
+                flag = jnp.where(j < blocks_of[qi], 1, 0)
+                found.append((qi, j, flag, count))
+                count = count + flag
+        units = count * heads
 
         def place(u):
-            u = jnp.minimum(u, units - 1)
-            qi = jnp.where(u >= split, 1, 0)
-            r = u - qi * split
-            return qi, zz * 4 + r // heads, r % heads
-
-        def finish(u, qi):
-            _, j, h = place(u)
-            spread(pbuf[...], abuf[...], qi, j, h, 1, False)
-
-        def one_unit(u, _):
-            qi, j, h = place(u)
-            before_qi = jnp.where(u > 0, place(jnp.maximum(u - 1, 0))[0], 2)
-            finish(jnp.maximum(u - 1, 0), before_qi)
-            later = scores(qi, j, h, 1, False)
-            w, alpha = soften(sbuf[...], qi, j, h, 0, False)
-            spread(w, alpha, qi, j, h, 0, False)
-            ahead = scores(*place(u + 1), 0, False)
-            w, alpha = soften(later, qi, j, h, 1, False)
-            sbuf[...] = ahead
+            v = jnp.clip(u, 0, units - 1)
+            k = v // heads
+            hits = [(qi, j, jnp.where(before_ == k, flag, 0)) for qi, j, flag, before_ in found]
+            qi = sum(hit * qi for qi, _, hit in hits)
+            j = sum(hit * j for _, j, hit in hits)
+            return jnp.where(u == v, qi, 2), j, v % heads
+
+        def two_units(i, _):
+            spread(pbuf[...], abuf[...], *place(2 * i - 1), 1, False)
+            here = held()
+            for t in range(4):
+                now = place(2 * i + t // 2)
+                ahead = scores(*place(2 * i + (t + 1) // 2), (t + 1) % 2, False)
+                w, alpha = soften(*here, *now, t % 2)
+                if t < 3:
+                    spread(w, alpha, *now, t % 2, False)
+                here = ahead
+            hold(*here)
             pbuf[...] = w
             abuf[...] = alpha
             return 0
 
         @pl.when(units > 0)
         def _():
-            sbuf[...] = scores(*place(0), 0, False)
-            lax.fori_loop(0, units, one_unit, 0)
-            finish(units - 1, place(units - 1)[0])
-
-        def for_queries(qi, _):
-            qblk = jnp.where(qi == 0, sp, pair_sp)
-
-            @pl.when(qblk // 4 == zz)
-            def _():
-                def for_head(h, _):
-                    tiles(qi, qblk, h, True)
-                    return 0
-
-                lax.fori_loop(0, heads, for_head, 0)
-
-            return 0
-
-        lax.fori_loop(0, 2, for_queries, 0)
-
-    def pass_on(tag, name, from_z, dev, landing_z):
+            hold(*scores(*place(0), 0, False))
+            steps = (units + 1) // 2
+            lax.fori_loop(0, steps, two_units, 0)
+            spread(pbuf[...], abuf[...], *place(2 * steps - 1), 1, False)
+
+        @pl.when((step == 0) | (step == 2 + z % 2))
+        def _():
+            qi = jnp.where(step == 0, 0, 1)
+
+            def for_head(h, _):
+                tiles(qi, jnp.where(step == 0, sp, pair_sp), h, True)
+                return 0
+
+            lax.fori_loop(0, heads, for_head, 0)
+
+    def pass_on(tag, name, from_z, dev, landing_z, sends, receives):
         col = cols[tag]
 
         def ends():
             src = kvbuf.at[from_z * 4 + col]
             return src, src, dev, kvbuf.at[landing_z * 4 + col]
 
-        send(name + tag, ends)
+        send(name + tag, ends, sends, receives)
 
     m_d, m_u, m_f = yd * 2 + c, yu * 2 + c, yf * 2 + c
     s_d, s_u, s_f = yd * 2 + 1 - c, yu * 2 + 1 - c, yf * 2 + 1 - c
 
-    def pass_x2(tag, zz, name, col, dev, start=0, size=WROWS):
+    def pass_x2(tag, zz, name, col, dev, start=0, size=UP):
         def ends():
-            src = weights(zz * 4 + col, start, size)
-            return src, src, dev, weights(zz * 4 + xf, start, size)
+            src = up_block(zz * 4 + col, start, size)
+            return src, src, dev, up_block(zz * 4 + xf, start, size)
 
         send(name + tag, ends)
 
-    def one_row(step, _):
-        offset = jnp.where(step == 1, 3, jnp.where(step == 2, 1, jnp.where(step == 3, 2, 0)))
-        attend_row((z + offset) % 4)
-
-        @pl.when(step == 0)
-        def _():
+    uhalf = UP // 2
+
+    def one_step(step, _):
+        attend(step)
+
+        @pl.when(step == 1)
+        def _():
+            take("wz1u", "wz1d")
+            pass_x("d", zd)
+            pass_x("u", zu)
             take("y1u", "y1d")
             send("y2u", lambda: (mix_rows(m_d, 0, 128), mix_rows(m_d, 0, 128), y_up, mix_rows(m_f, 0, 128)))
             send("y2d", lambda: (mix_rows(m_u, 128, 128), mix_rows(m_u, 128, 128), y_down, mix_rows(m_f, 128, 128)))
             send("s1", lambda: (mix_rows(m_d), mix_rows(m_d), sibling, mix_rows(s_d)))
             send("s2", lambda: (mix_rows(m_u), mix_rows(m_u), sibling, mix_rows(s_u)))
-            take("z1u_own", "z1d_own", "z1u_mate", "z1d_mate")
-            pass_on("own", "z2u_", zd, above, zf)
-            pass_on("mate", "z2u_", zd, above, zf)
+            take("z1u_mate", "z1d_mate")
+            pass_on("mate", "z2u_", zd, above, zf, lambda: z >= 1, lambda: z != 1)
             take("z1u_opp", "z1d_opp", "z1u_diag", "z1d_diag")
-            pass_on("opp", "z2d_", zu, below, zf)
-            pass_on("diag", "z2d_", zu, below, zf)
+            pass_on("opp", "z2d_", zu, below, zf, lambda: z != 2, lambda: z != 1)
+            pass_on("diag", "z2d_", zu, below, zf, lambda: z != 2, lambda: z != 1)
+            send("wz2u", lambda: (up_block(b_d, 0, uhalf), up_block(b_d, 0, uhalf), above, up_block(b_f, 0, uhalf)))
+            send("wz2d", lambda: (up_block(b_u, uhalf, uhalf), up_block(b_u, uhalf, uhalf), below, up_block(b_f, uhalf, uhalf)))
+            take("wx1r0", "wx1l0")
+            pass_x2("0", z, "wx2r", xl, right)
+
+        @pl.when(step == 2)
+        def _():
+            take("z2u_own", "z2x_own")
+            take("wx1rd", "wx1ld", "wx1ru", "wx1lu")
+            pass_x2("d", zd, "wx2l", xr, left)
+            pass_x2("u", zu, "wx2r", xl, right, 0, uhalf)
+            pass_x2("u", zu, "wx2l", xr, left, uhalf, uhalf)
+
+        @pl.when(step == 3)
+        def _():
+            take("y2u", "y2d")
+            send("s3", lambda: (mix_rows(m_f), mix_rows(m_f), sibling, mix_rows(s_f)))
             take("wz2u", "wz2d")
             pass_x("f", zf)
-            take("wx1r0", "wx1l0")
-            pass_x2("0", z, "wx2r", xl, right)
-
-        @pl.when(step == 1)
-        def _():
-            take("wx1rd", "wx1ld", "wx1ru", "wx1lu")
-            pass_x2("d", zd, "wx2l", xr, left)
-            pass_x2("u", zu, "wx2r", xl, right, 0, WHALF)
-            pass_x2("u", zu, "wx2l", xr, left, WHALF, WHALF)
-
-        @pl.when(step == 2)
-        def _():
-            take("y2u", "y2d")
-            send("s3", lambda: (mix_rows(m_f), mix_rows(m_f), sibling, mix_rows(s_f)))
-            take("wx1rf", "wx1lf")
-            pass_x2("f", zf, "wx2r", xl, right, 0, WHALF)
-            pass_x2("f", zf, "wx2l", xr, left, WHALF, WHALF)
-            take("z2u_own", "z2u_mate", "z2d_opp", "z2d_diag")
+            take("z2u_mate", "z2d_opp", "z2d_diag")
+            take("bx2r", "bx2l")
+            send("bz1u", lambda: (down_blocks(z * 4, 4), down_blocks(z * 4, 4), above, down_blocks(zd * 4, 4)))
+            send("bz1d", lambda: (down_blocks(z * 4, 4), down_blocks(z * 4, 4), below, down_blocks(zu * 4, 4)))
 
         return 0
 
-    lax.fori_loop(0, 4, one_row, 0)
+    lax.fori_loop(0, 5, one_step, 0)
 
     keep0 = head_lanes(0)
     for qi in (1, 0):
@@ -464,6 +512,9 @@
 
     for d in range(8):
         send_out(d)
+    take("wx1rf", "wx1lf")
+    pass_x2("f", zf, "wx2r", xl, right, 0, uhalf)
+    pass_x2("f", zf, "wx2l", xr, left, uhalf, uhalf)
     arrived[slot] = outv[0, own_rows(tp), :]
     take("s0", "s1", "s2", "s3")
     for d in range(8):
@@ -500,6 +551,9 @@
     send("gu", lambda: (rows_of(tp), rows_of(tp), y_up, rows_of(m_d)))
     send("gd", lambda: (rows_of(tp), rows_of(tp), y_down, rows_of(m_u)))
     send("gs", lambda: (rows_of(tp), rows_of(tp), sibling, rows_of(y * 2 + 1 - c)))
+    take("bz1u", "bz1d")
+    send("bz2u", lambda: (down_blocks(zd * 4, 2), down_blocks(zd * 4, 2), above, down_blocks(zf * 4, 2)))
+    send("bz2d", lambda: (down_blocks(zu * 4 + 2, 2), down_blocks(zu * 4 + 2, 2), below, down_blocks(zf * 4 + 2, 2)))
     take("wx2r0", "wx2ld", "wx2ru", "wx2lu", "wx2rf", "wx2lf")
 
     def up_group(*chips):
@@ -521,8 +575,30 @@
         lax.fori_loop(0, 5, chunk, 0)
         some(1280, 128)
 
+    def send_halo():
+        pltpu.make_async_remote_copy(
+            src_ref=both.at[pl.ds(BLK, 16)],
+            dst_ref=halo,
+            send_sem=ssem.at[HALO_SEM],
+            recv_sem=rsem.at[HALO_SEM],
+            device_id=after,
+            device_id_type=MESH,
+        ).start()
+
+    def wait_halo(which):
+        copy = pltpu.make_async_remote_copy(
+            src_ref=both.at[pl.ds(BLK, 16)],
+            dst_ref=halo,
+            send_sem=ssem.at[HALO_SEM],
+            recv_sem=rsem.at[HALO_SEM],
+            device_id=after,
+            device_id_type=MESH,
+        )
+        copy.wait_recv() if which else copy.wait_send()
+
     take("gs")
     up_group(y)
+    pl.when(y == 3)(send_halo)
     take("gu", "gd")
     send("g2u", lambda: (rows_of(m_d, 0, 48), rows_of(m_d, 0, 48), y_up, rows_of(m_f, 0, 48)))
     send("g2d", lambda: (rows_of(m_u, 48, 48), rows_of(m_u, 48, 48), y_down, rows_of(m_f, 48, 48)))
@@ -530,11 +606,12 @@
     send("gs2", lambda: (rows_of(m_u), rows_of(m_u), sibling, rows_of(s_u)))
     take("gs1", "gs2")
     up_group(yd, yu)
+    pl.when((yd == 3) | (yu == 3))(send_halo)
     take("g2u", "g2d")
     send("gs3", lambda: (rows_of(m_f), rows_of(m_f), sibling, rows_of(s_f)))
     take("gs3")
     up_group(yf)
-    send("halo", lambda: (both.at[pl.ds(BLK, 16)], halo, after, halo))
+    pl.when(yf == 3)(send_halo)
 
     taps[0:3, 0:640] = vtaps_ref[:, 0:640]
     taps[0:3, 640:1280] = gtaps_ref[:, 0:640]
@@ -565,16 +642,17 @@
                 value = jnp.where(lane < 64, value, 0.0)
             hid[dst, g * 128 : (g + 1) * 128] = value.astype(BF16)
 
-    def hidden_step(i, _):
-        @pl.when(i == 7)
-        def _():
-            take("halo")
+    def hidden_group(yy):
+        @pl.when(yy == 0)
+        def _():
+            wait_halo(True)
             both[0:16, :] = jnp.where(sp == 0, 0.0, halo[...].astype(F32)).astype(BF16)
 
-        hidden_rows((i + 1) % 8)
-        return 0
-
-    lax.fori_loop(0, 8, hidden_step, 0)
+        def chunk(i, _):
+            hidden_rows(yy * 2 + i)
+            return 0
+
+        lax.fori_loop(0, 2, chunk, 0)
 
     def down_group(g, yy):
         mine = hid[pl.ds(pl.multiple_of(yy * 192 + c * OWN, 32), OWN), :]
@@ -599,46 +677,70 @@
     def pair_sum(g, lo, hi):
         return keep[g, :, lo:hi] + sib_in[g, :, lo:hi].astype(F32)
 
-    down_group(0, yf)
-    send_sib(0)
-    down_group(1, yd)
-    send_sib(1)
-    take("r0")
-    far_out[0] = pair_sum(0, 0, HALF).astype(BF16)
-    far_out[1] = pair_sum(0, HALF, 2 * HALF).astype(BF16)
-    send("fu", lambda: (far_out.at[0], far_in.at[0], y_up, far_in.at[0]))
-    send("fd", lambda: (far_out.at[1], far_in.at[1], y_down, far_in.at[1]))
-    down_group(2, yu)
-    send_sib(2)
-    down_group(3, y)
-    send_sib(3)
-    take("r1", "r2")
-    near_out[0, :, HALF:] = pair_sum(2, HALF, 2 * HALF).astype(BF16)
-    near_out[1, :, :HALF] = pair_sum(1, 0, HALF).astype(BF16)
+    take("bz2u", "bz2d")
+
+    def near(k, h):
+        send(
+            "n%d%d" % (k, h),
+            lambda: (near_out.at[k, h], near_in.at[k, h], (y_up, y_down)[k], near_in.at[k, h]),
+        )
+
+    def ffn_step(g, _):
+        yy = (y + jnp.where(g == 0, 2, jnp.where(g == 1, 3, jnp.where(g == 2, 1, 0)))) % 4
+        hidden_group(yy)
+        down_group(g, yy)
+
+        @pl.when(g == 0)
+        def _():
+            send_sib(0)
+
+        @pl.when(g == 1)
+        def _():
+            send_sib(1)
+            take("r0")
+            far_out[0] = pair_sum(0, 0, HALF).astype(BF16)
+            far_out[1] = pair_sum(0, HALF, 2 * HALF).astype(BF16)
+            send("fu", lambda: (far_out.at[0], far_in.at[0], y_up, far_in.at[0]))
+            send("fd", lambda: (far_out.at[1], far_in.at[1], y_down, far_in.at[1]))
+
+        @pl.when(g == 2)
+        def _():
+            send_sib(2)
+            take("r1")
+            near_out[1, 0] = pair_sum(1, 0, HALF).astype(BF16)
+            near(1, 0)
+
+        @pl.when(g == 3)
+        def _():
+            send_sib(3)
+            take("r2")
+            near_out[0, 1] = pair_sum(2, HALF, 2 * HALF).astype(BF16)
+            near(0, 1)
+
+        return 0
+
+    lax.fori_loop(0, 4, ffn_step, 0)
     take("fu")
-    near_out[0, :, :HALF] = (pair_sum(2, 0, HALF) + far_in[0].astype(F32)).astype(BF16)
-    send("nu", lambda: (near_out.at[0], near_in.at[0], y_up, near_in.at[0]))
+    near_out[0, 0] = (pair_sum(2, 0, HALF) + far_in[0].astype(F32)).astype(BF16)
+    near(0, 0)
     take("fd")
-    near_out[1, :, HALF:] = (pair_sum(1, HALF, 2 * HALF) + far_in[1].astype(F32)).astype(BF16)
-    send("nd", lambda: (near_out.at[1], near_in.at[1], y_down, near_in.at[1]))
-    take("r3", "nu", "nd")
+    near_out[1, 1] = (pair_sum(1, HALF, 2 * HALF) + far_in[1].astype(F32)).astype(BF16)
+    near(1, 1)
+    take("r3", "n00", "n01", "n10", "n11")
 
     def last_norm(i, _):
         r = pl.ds(pl.multiple_of(i * 16, 16), 16)
         t = pl.ds(pl.multiple_of(tp * OWN + i * 16, 16), 16)
-        ffn = (
-            keep[3, r, :]
-            + sib_in[3, r, :].astype(F32)
-            + near_in[0, r, :].astype(F32)
-            + near_in[1, r, :].astype(F32)
-        )
+        far = [near_in[0, h, r, :].astype(F32) + near_in[1, h, r, :].astype(F32) for h in range(2)]
+        ffn = keep[3, r, :] + sib_in[3, r, :].astype(F32) + jnp.concatenate(far, axis=1)
         whole = residual_scale * mixed[t, :].astype(F32) + ffn
         out_ref[r, :] = norm(whole, fgain_ref[...]).astype(BF16)
         return 0
 
     lax.fori_loop(0, OWN // 16, last_norm, 0)
-    for copy in sent:
-        copy(False).wait_send()
+    wait_halo(False)
+    for wait in sent:
+        wait()
 
 
 def whole_layer(*operands):
@@ -654,13 +756,14 @@
             pltpu.VMEM((16, BLK + EXTRA, 256), BF16),
             pltpu.VMEM((BLK, 128), BF16),
             pltpu.VMEM((EXTRA, 256), BF16),
-            pltpu.VMEM((2, 2, BLK, 128), BF16),
-            pltpu.VMEM((2, 2, BLK, 128), F32),
+            pltpu.VMEM((3, 2, BLK, 128), BF16),
+            pltpu.VMEM((3, 2, BLK, 128), F32),
             pltpu.VMEM((32, 8, BLK), F32),
-            pltpu.VMEM((2, 2, BLK, 128), F32),
-            pltpu.VMEM((2, 2, BLK, 128), F32),
+            pltpu.VMEM((3, 2, BLK, 128), F32),
+            pltpu.VMEM((3, 2, BLK, 128), F32),
             pltpu.VMEM((3, BLK, 128), F32),
             pltpu.VMEM((RQ, BLK), F32),
+            pltpu.VMEM((RQ, 128), F32),
             pltpu.VMEM((RQ, BLK), BF16),
             pltpu.VMEM((RQ, 128), F32),
             pltpu.VMEM((2, BLK, 128), BF16),
@@ -678,8 +781,8 @@
             pltpu.VMEM((4, OWN, 2048), BF16),
             pltpu.VMEM((2, OWN, HALF), BF16),
             pltpu.VMEM((2, OWN, HALF), BF16),
-            pltpu.VMEM((2, OWN, 2048), BF16),
-            pltpu.VMEM((2, OWN, 2048), BF16),
+            pltpu.VMEM((2, 2, OWN, HALF), BF16),
+            pltpu.VMEM((2, 2, OWN, HALF), BF16),
             pltpu.SemaphoreType.DMA((112,)),
             pltpu.SemaphoreType.DMA((112,)),
             pltpu.SemaphoreType.DMA((2,)),

time: 175 us -> 157 us (0.90)
  Pallas kernels: 170 us -> 153 us
    pallas_call x1, Pallas kernels: 170 us -> 153 us  [whole_layer(): pl.pallas_call(layer_kernel, out_shape=jax.ShapeDtypeStruct((OWN, 2048),...]
where the time goes in v4:
time: 157 us; the launch traced here: 155 us
  Pallas kernels  153 us (97%)
  local copies, waits for them, and re-layouts  1.77 us (1%)
    pallas_call x1, Pallas kernels, whole_layer(): pl.pallas_call(layer_kernel, out_shape=jax.ShapeDtypeStruct((OWN, 2048),...  153 us

profile of v4, /device:TPU:1, one launch (start us, length us, event | category | flops | bytes accessed | tf_op | source)
XLA Modules:
  0.0 154.6 jit_solution(16035329732064186971)
XLA Ops:
  0.0 152.8 %shard_map.172 = bf16[96,2048]{1,0:T(8,128)(2,1)} custom-call(bf16[768,128]{1,0:T(8,128)(2,1)} %qs_ref.1, bf16[768,128]{1,0:T(8,128)(2,1)} %ks_ref.1, bf16[768,128]{1,0:T(8,128)(2,1)} %vs_ref.1, bf16[768,128]{1,0:T(8,128)(2,1)} %ql_ref.1, bf16[768,128]{1,0:T(8,128)(2,1)} %kl_ref.1, bf16[768,128]{1,0:T(8,128)(2,1)} %vl_ref.1, f32[2,768]{1,0:T(2,128)} %bitcast.10, ...), custom_call_target="tpu_custom_call" | custom-call | flops 20000000000 | bytes 40000000 | tf_op jit(solution)/shard_map/pallas_call | solution.py:748
  152.8 1.8 %copy.20 = bf16[96,2048]{1,0:T(8,128)(2,1)} copy(bf16[96,2048]{1,0:T(8,128)(2,1)} %shard_map.172) | data formatting | bytes 786432

commit v5 on v4

--- a/solution.py
+++ b/solution.py
@@ -163,7 +163,7 @@
     counter = [0]
     incoming = {}
 
-    def send(name, ends, sends=None, receives=None):
+    def send(name, ends, sends=None, receives=None, now=None):
         k = counter[0]
         counter[0] += 1
 
@@ -183,7 +183,7 @@
 
         sent.append(lambda: only(sends, lambda: copy(False).wait_send()))
         incoming[name] = lambda: only(receives, lambda: copy(True).wait_recv())
-        only(sends, lambda: copy(False).start())
+        only(now or sends, lambda: copy(False).start())
         return lambda: copy(False).start()
 
     def take(*names):
@@ -431,14 +431,25 @@
     m_d, m_u, m_f = yd * 2 + c, yu * 2 + c, yf * 2 + c
     s_d, s_u, s_f = yd * 2 + 1 - c, yu * 2 + 1 - c, yf * 2 + 1 - c
 
-    def pass_x2(tag, zz, name, col, dev, start=0, size=UP):
+    def pass_x2(tag, zz, name, col, dev, start=0, size=UP, now=None):
         def ends():
             src = up_block(zz * 4 + col, start, size)
             return src, src, dev, up_block(zz * 4 + xf, start, size)
 
-        send(name + tag, ends)
+        return send(name + tag, ends, now=now)
 
     uhalf = UP // 2
+
+    def both_ways(tag, zz):
+        pass_x2(tag, zz, "wx2r", xl, right, 0, uhalf)
+        pass_x2(tag, zz, "wx2l", xr, left, uhalf, uhalf)
+
+    def down_pair(name, zz, first, dev, landing):
+        def ends():
+            src = down_blocks(zz * 4 + first, 2)
+            return src, src, dev, down_blocks(landing * 4 + first, 2)
+
+        send(name, ends)
 
     def one_step(step, _):
         attend(step)
@@ -446,6 +457,8 @@
         @pl.when(step == 1)
         def _():
             take("wz1u", "wz1d")
+            send("wz2u", lambda: (up_block(b_d, 0, uhalf), up_block(b_d, 0, uhalf), above, up_block(b_f, 0, uhalf)))
+            send("wz2d", lambda: (up_block(b_u, uhalf, uhalf), up_block(b_u, uhalf, uhalf), below, up_block(b_f, uhalf, uhalf)))
             pass_x("d", zd)
             pass_x("u", zu)
             take("y1u", "y1d")
@@ -458,29 +471,29 @@
             take("z1u_opp", "z1d_opp", "z1u_diag", "z1d_diag")
             pass_on("opp", "z2d_", zu, below, zf, lambda: z != 2, lambda: z != 1)
             pass_on("diag", "z2d_", zu, below, zf, lambda: z != 2, lambda: z != 1)
-            send("wz2u", lambda: (up_block(b_d, 0, uhalf), up_block(b_d, 0, uhalf), above, up_block(b_f, 0, uhalf)))
-            send("wz2d", lambda: (up_block(b_u, uhalf, uhalf), up_block(b_u, uhalf, uhalf), below, up_block(b_f, uhalf, uhalf)))
             take("wx1r0", "wx1l0")
-            pass_x2("0", z, "wx2r", xl, right)
+            both_ways("0", z)
 
         @pl.when(step == 2)
         def _():
             take("z2u_own", "z2x_own")
+            take("wz2u", "wz2d")
+            pass_x("f", zf)
+
+        @pl.when(step == 2)
+        def _():
             take("wx1rd", "wx1ld", "wx1ru", "wx1lu")
-            pass_x2("d", zd, "wx2l", xr, left)
-            pass_x2("u", zu, "wx2r", xl, right, 0, uhalf)
-            pass_x2("u", zu, "wx2l", xr, left, uhalf, uhalf)
+            both_ways("d", zd)
+            both_ways("u", zu)
 
         @pl.when(step == 3)
         def _():
             take("y2u", "y2d")
             send("s3", lambda: (mix_rows(m_f), mix_rows(m_f), sibling, mix_rows(s_f)))
-            take("wz2u", "wz2d")
-            pass_x("f", zf)
             take("z2u_mate", "z2d_opp", "z2d_diag")
             take("bx2r", "bx2l")
-            send("bz1u", lambda: (down_blocks(z * 4, 4), down_blocks(z * 4, 4), above, down_blocks(zd * 4, 4)))
-            send("bz1d", lambda: (down_blocks(z * 4, 4), down_blocks(z * 4, 4), below, down_blocks(zu * 4, 4)))
+            down_pair("bz1u", z, 0, above, zd)
+            down_pair("bz1d", z, 2, below, zu)
 
         return 0
 
@@ -512,9 +525,18 @@
 
     for d in range(8):
         send_out(d)
-    take("wx1rf", "wx1lf")
-    pass_x2("f", zf, "wx2r", xl, right, 0, uhalf)
-    pass_x2("f", zf, "wx2l", xr, left, uhalf, uhalf)
+    far_waits = [incoming.pop("wx1rf"), incoming.pop("wx1lf")]
+    is_large = lambda: role == 1
+
+    @pl.when(role == 1)
+    def _():
+        for wait in far_waits:
+            wait()
+
+    far_sends = [
+        pass_x2("f", zf, "wx2r", xl, right, 0, uhalf, is_large),
+        pass_x2("f", zf, "wx2l", xr, left, uhalf, uhalf, is_large),
+    ]
     arrived[slot] = outv[0, own_rows(tp), :]
     take("s0", "s1", "s2", "s3")
     for d in range(8):
@@ -522,6 +544,19 @@
         if d:
             take("a%d" % d)
 
+    @pl.when(role == 0)
+    def _():
+        for wait in far_waits:
+            wait()
+        for start in far_sends:
+            start()
+
+    take("bz1u", "bz1d")
+    down_pair("bz2u", zd, 0, above, zf)
+    down_pair("bz2d", zu, 2, below, zf)
+    down_pair("bz3u", z, 2, above, zd)
+    down_pair("bz3d", z, 0, below, zu)
+
     def project(i, _):
         col = pl.ds(pl.multiple_of(i * 256, 256), 256)
         lhs = jnp.concatenate([arrived[s] for s in range(16)], axis=1)
@@ -551,10 +586,7 @@
     send("gu", lambda: (rows_of(tp), rows_of(tp), y_up, rows_of(m_d)))
     send("gd", lambda: (rows_of(tp), rows_of(tp), y_down, rows_of(m_u)))
     send("gs", lambda: (rows_of(tp), rows_of(tp), sibling, rows_of(y * 2 + 1 - c)))
-    take("bz1u", "bz1d")
-    send("bz2u", lambda: (down_blocks(zd * 4, 2), down_blocks(zd * 4, 2), above, down_blocks(zf * 4, 2)))
-    send("bz2d", lambda: (down_blocks(zu * 4 + 2, 2), down_blocks(zu * 4 + 2, 2), below, down_blocks(zf * 4 + 2, 2)))
-    take("wx2r0", "wx2ld", "wx2ru", "wx2lu", "wx2rf", "wx2lf")
+    take("wx2r0", "wx2l0", "wx2rd", "wx2ld", "wx2ru", "wx2lu", "wx2rf", "wx2lf")
 
     def up_group(*chips):
         def some(start, width):
@@ -595,23 +627,6 @@
             device_id_type=MESH,
         )
         copy.wait_recv() if which else copy.wait_send()
-
-    take("gs")
-    up_group(y)
-    pl.when(y == 3)(send_halo)
-    take("gu", "gd")
-    send("g2u", lambda: (rows_of(m_d, 0, 48), rows_of(m_d, 0, 48), y_up, rows_of(m_f, 0, 48)))
-    send("g2d", lambda: (rows_of(m_u, 48, 48), rows_of(m_u, 48, 48), y_down, rows_of(m_f, 48, 48)))
-    send("gs1", lambda: (rows_of(m_d), rows_of(m_d), sibling, rows_of(s_d)))
-    send("gs2", lambda: (rows_of(m_u), rows_of(m_u), sibling, rows_of(s_u)))
-    take("gs1", "gs2")
-    up_group(yd, yu)
-    pl.when((yd == 3) | (yu == 3))(send_halo)
-    take("g2u", "g2d")
-    send("gs3", lambda: (rows_of(m_f), rows_of(m_f), sibling, rows_of(s_f)))
-    take("gs3")
-    up_group(yf)
-    pl.when(yf == 3)(send_halo)
 
     taps[0:3, 0:640] = vtaps_ref[:, 0:640]
     taps[0:3, 640:1280] = gtaps_ref[:, 0:640]
@@ -677,49 +692,53 @@
     def pair_sum(g, lo, hi):
         return keep[g, :, lo:hi] + sib_in[g, :, lo:hi].astype(F32)
 
-    take("bz2u", "bz2d")
-
     def near(k, h):
         send(
             "n%d%d" % (k, h),
             lambda: (near_out.at[k, h], near_in.at[k, h], (y_up, y_down)[k], near_in.at[k, h]),
         )
 
-    def ffn_step(g, _):
-        yy = (y + jnp.where(g == 0, 2, jnp.where(g == 1, 3, jnp.where(g == 2, 1, 0)))) % 4
-        hidden_group(yy)
-        down_group(g, yy)
-
-        @pl.when(g == 0)
-        def _():
-            send_sib(0)
-
-        @pl.when(g == 1)
-        def _():
-            send_sib(1)
-            take("r0")
-            far_out[0] = pair_sum(0, 0, HALF).astype(BF16)
-            far_out[1] = pair_sum(0, HALF, 2 * HALF).astype(BF16)
-            send("fu", lambda: (far_out.at[0], far_in.at[0], y_up, far_in.at[0]))
-            send("fd", lambda: (far_out.at[1], far_in.at[1], y_down, far_in.at[1]))
-
-        @pl.when(g == 2)
-        def _():
-            send_sib(2)
-            take("r1")
-            near_out[1, 0] = pair_sum(1, 0, HALF).astype(BF16)
-            near(1, 0)
-
-        @pl.when(g == 3)
-        def _():
-            send_sib(3)
-            take("r2")
-            near_out[0, 1] = pair_sum(2, HALF, 2 * HALF).astype(BF16)
-            near(0, 1)
-
-        return 0
-
-    lax.fori_loop(0, 4, ffn_step, 0)
+    take("gs")
+    up_group(y)
+    pl.when(y == 3)(send_halo)
+    take("gu", "gd")
+    send("g2u", lambda: (rows_of(m_d, 0, 48), rows_of(m_d, 0, 48), y_up, rows_of(m_f, 0, 48)))
+    send("g2d", lambda: (rows_of(m_u, 48, 48), rows_of(m_u, 48, 48), y_down, rows_of(m_f, 48, 48)))
+    send("gs1", lambda: (rows_of(m_d), rows_of(m_d), sibling, rows_of(s_d)))
+    send("gs2", lambda: (rows_of(m_u), rows_of(m_u), sibling, rows_of(s_u)))
+    take("gs1", "gs2")
+    up_group(yd, yu)
+    pl.when((yd == 3) | (yu == 3))(send_halo)
+    take("g2u", "g2d")
+    send("gs3", lambda: (rows_of(m_f), rows_of(m_f), sibling, rows_of(s_f)))
+    take("bz2u", "bz2d", "bz3u", "bz3d")
+    hidden_group(yu)
+    down_group(2, yu)
+    send_sib(2)
+    take("gs3")
+    up_group(yf)
+    pl.when(yf == 3)(send_halo)
+    take("r2")
+    near_out[0, 1] = pair_sum(2, HALF, 2 * HALF).astype(BF16)
+    near(0, 1)
+    hidden_group(yf)
+    down_group(0, yf)
+    send_sib(0)
+    hidden_group(yd)
+    take("r0")
+    far_out[0] = pair_sum(0, 0, HALF).astype(BF16)
+    far_out[1] = pair_sum(0, HALF, 2 * HALF).astype(BF16)
+    send("fu", lambda: (far_out.at[0], far_in.at[0], y_up, far_in.at[0]))
+    send("fd", lambda: (far_out.at[1], far_in.at[1], y_down, far_in.at[1]))
+    down_group(1, yd)
+    send_sib(1)
+    hidden_group(y)
+    take("r1")
+    near_out[1, 0] = pair_sum(1, 0, HALF).astype(BF16)
+    near(1, 0)
+    down_group(3, y)
+    send_sib(3)
+
     take("fu")
     near_out[0, 0] = (pair_sum(2, 0, HALF) + far_in[0].astype(F32)).astype(BF16)
     near(0, 0)

time: 157 us -> 151 us (0.962)
  Pallas kernels: 153 us -> 148 us
    pallas_call x1, Pallas kernels: 153 us -> 148 us  [whole_layer(): pl.pallas_call(layer_kernel, out_shape=jax.ShapeDtypeStruct((OWN, 2048),...]
where the time goes in v5:
time: 151 us; the launch traced here: 150 us
  Pallas kernels  148 us (98%)
  local copies, waits for them, and re-layouts  1.77 us (1%)
    pallas_call x1, Pallas kernels, whole_layer(): pl.pallas_call(layer_kernel, out_shape=jax.ShapeDtypeStruct((OWN, 2048),...  148 us

profile of v5, /device:TPU:1, one launch (start us, length us, event | category | flops | bytes accessed | tf_op | source)
XLA Modules:
  0.0 149.8 jit_solution(12240700386131426553)
XLA Ops:
  0.0 148.0 %shard_map.172 = bf16[96,2048]{1,0:T(8,128)(2,1)} custom-call(bf16[768,128]{1,0:T(8,128)(2,1)} %qs_ref.1, bf16[768,128]{1,0:T(8,128)(2,1)} %ks_ref.1, bf16[768,128]{1,0:T(8,128)(2,1)} %vs_ref.1, bf16[768,128]{1,0:T(8,128)(2,1)} %ql_ref.1, bf16[768,128]{1,0:T(8,128)(2,1)} %kl_ref.1, bf16[768,128]{1,0:T(8,128)(2,1)} %vl_ref.1, f32[2,768]{1,0:T(2,128)} %bitcast.10, ...), custom_call_target="tpu_custom_call" | custom-call | flops 20000000000 | bytes 40000000 | tf_op jit(solution)/shard_map/pallas_call | solution.py:767
  148.0 1.8 %copy.20 = bf16[96,2048]{1,0:T(8,128)(2,1)} copy(bf16[96,2048]{1,0:T(8,128)(2,1)} %shard_map.172) | data formatting | bytes 786432

commit v6 on v5

--- a/solution.py
+++ b/solution.py
@@ -558,13 +558,13 @@
     down_pair("bz3d", z, 0, below, zu)
 
     def project(i, _):
-        col = pl.ds(pl.multiple_of(i * 256, 256), 256)
+        col = pl.ds(pl.multiple_of(i * 1024, 1024), 1024)
         lhs = jnp.concatenate([arrived[s] for s in range(16)], axis=1)
         part = jnp.dot(lhs, mixbuf[:, col], preferred_element_type=F32)
         ybuf[:, col] = residual_scale * res_ref[:, col].astype(F32) + part
         return 0
 
-    lax.fori_loop(0, 8, project, 0)
+    lax.fori_loop(0, 2, project, 0)
 
     def norm(values, gain):
         center = jnp.mean(values, axis=1, keepdims=True)
@@ -573,12 +573,12 @@
         return off * lax.rsqrt(spread + epsilon) * gain
 
     def first_norm(i, _):
-        r = pl.ds(pl.multiple_of(i * 16, 16), 16)
-        t = pl.ds(pl.multiple_of(tp * OWN + i * 16, 16), 16)
+        r = pl.ds(pl.multiple_of(i * 48, 48), 48)
+        t = pl.ds(pl.multiple_of(tp * OWN + i * 48, 48), 48)
         mixed[t, :] = norm(ybuf[r, :], mgain_ref[...]).astype(BF16)
         return 0
 
-    lax.fori_loop(0, OWN // 16, first_norm, 0)
+    lax.fori_loop(0, OWN // 48, first_norm, 0)
 
     def rows_of(t, start=0, size=OWN):
         return mixed.at[pl.ds(pl.multiple_of(t * OWN + start, 16), size)]
@@ -600,12 +600,7 @@
                 into = pl.ds(pl.multiple_of(yy * 192 + 16, 16), 192)
                 both[into, cols_] = part[k * 192 : (k + 1) * 192]
 
-        def chunk(i, _):
-            some(pl.multiple_of(i * 256, 256), 256)
-            return 0
-
-        lax.fori_loop(0, 5, chunk, 0)
-        some(1280, 128)
+        some(0, UP)
 
     def send_halo():
         pltpu.make_async_remote_copy(
@@ -675,16 +670,14 @@
         lhs = jnp.concatenate([mine, other], axis=0)
 
         def some(i, _):
-            col = pl.ds(pl.multiple_of(i * 256, 256), 256)
-            rhs = jnp.concatenate(
-                [wbuf[2 * i, 1408 : WROWS + 64, :], wbuf[2 * i + 1, 1408 : WROWS + 64, :]], axis=1
-            )
+            col = pl.ds(pl.multiple_of(i * 1024, 1024), 1024)
+            rhs = jnp.concatenate([wbuf[8 * i + k, 1408 : WROWS + 64, :] for k in range(8)], axis=1)
             part = jnp.dot(lhs, rhs, preferred_element_type=F32)
             keep[g, :, col] = part[:OWN]
             sib_out[g, :, col] = part[OWN:].astype(BF16)
             return 0
 
-        lax.fori_loop(0, 8, some, 0)
+        lax.fori_loop(0, 2, some, 0)
 
     def send_sib(g):
         send("r%d" % g, lambda: (sib_out.at[g], sib_in.at[g], sibling, sib_in.at[g]))
@@ -748,15 +741,15 @@
     take("r3", "n00", "n01", "n10", "n11")
 
     def last_norm(i, _):
-        r = pl.ds(pl.multiple_of(i * 16, 16), 16)
-        t = pl.ds(pl.multiple_of(tp * OWN + i * 16, 16), 16)
+        r = pl.ds(pl.multiple_of(i * 48, 48), 48)
+        t = pl.ds(pl.multiple_of(tp * OWN + i * 48, 48), 48)
         far = [near_in[0, h, r, :].astype(F32) + near_in[1, h, r, :].astype(F32) for h in range(2)]
         ffn = keep[3, r, :] + sib_in[3, r, :].astype(F32) + jnp.concatenate(far, axis=1)
         whole = residual_scale * mixed[t, :].astype(F32) + ffn
         out_ref[r, :] = norm(whole, fgain_ref[...]).astype(BF16)
         return 0
 
-    lax.fori_loop(0, OWN // 16, last_norm, 0)
+    lax.fori_loop(0, OWN // 48, last_norm, 0)
     wait_halo(False)
     for wait in sent:
         wait()

time: 151 us -> 147 us (0.974)
  Pallas kernels: 148 us -> 145 us
    pallas_call x1, Pallas kernels: 148 us -> 145 us  [whole_layer(): pl.pallas_call(layer_kernel, out_shape=jax.ShapeDtypeStruct((OWN, 2048),...]
where the time goes in v6:
time: 147 us
  Pallas kernels  145 us (99%)
  local copies, waits for them, and re-layouts  1.77 us (1%)
    pallas_call x1, Pallas kernels, whole_layer(): pl.pallas_call(layer_kernel, out_shape=jax.ShapeDtypeStruct((OWN, 2048),...  145 us

profile of v6, /device:TPU:1, one launch (start us, length us, event | category | flops | bytes accessed | tf_op | source)
XLA Modules:
  0.0 146.8 jit_solution(5770442435515736919)
XLA Ops:
  0.0 145.0 %shard_map.172 = bf16[96,2048]{1,0:T(8,128)(2,1)} custom-call(bf16[768,128]{1,0:T(8,128)(2,1)} %qs_ref.1, bf16[768,128]{1,0:T(8,128)(2,1)} %ks_ref.1, bf16[768,128]{1,0:T(8,128)(2,1)} %vs_ref.1, bf16[768,128]{1,0:T(8,128)(2,1)} %ql_ref.1, bf16[768,128]{1,0:T(8,128)(2,1)} %kl_ref.1, bf16[768,128]{1,0:T(8,128)(2,1)} %vl_ref.1, f32[2,768]{1,0:T(2,128)} %bitcast.10, ...), custom_call_target="tpu_custom_call" | custom-call | flops 20000000000 | bytes 40000000 | tf_op jit(solution)/shard_map/pallas_call | solution.py:760
  145.0 1.8 %copy.20 = bf16[96,2048]{1,0:T(8,128)(2,1)} copy(bf16[96,2048]{1,0:T(8,128)(2,1)} %shard_map.172) | data formatting | bytes 786432

commit v7 on v6

--- a/solution.py
+++ b/solution.py
@@ -374,7 +374,7 @@
         found, count = [], 0
         for qi in range(2):
             for j in slots:
-                flag = jnp.where(j < blocks_of[qi], 1, 0)
+                flag = jnp.where((j < blocks_of[qi]) & (step != 4 + qi), 1, 0)
                 found.append((qi, j, flag, count))
                 count = count + flag
         units = count * heads
@@ -450,6 +450,28 @@
             return src, src, dev, down_blocks(landing * 4 + first, 2)
 
         send(name, ends)
+
+    keep0 = head_lanes(0)
+    slot = tp * 2 + role
+
+    def own_rows(t):
+        return pl.ds(pl.multiple_of(t * OWN, 32), OWN)
+
+    def finish_out(qi):
+        l0 = jnp.sum(lst[qi, 0], axis=1, keepdims=True)
+        l1 = jnp.sum(lst[qi, 1], axis=1, keepdims=True)
+        outv[qi] = (acc[qi] / jnp.where(keep0, l0, l1)).astype(BF16)
+
+    def send_out(name, qi, d):
+        def ends():
+            t, s = (tp + d) % 8, (tp + 8 - d) % 8
+            dev = ((sp, pair_sp)[qi], t // 2, t % 2)
+            from_role = (role, 1 - role)[qi]
+            return outv.at[qi, own_rows(t)], arrived.at[slot], dev, arrived.at[s * 2 + from_role]
+
+        send(name + "%d" % d, ends)
+
+    pair_sent = []
 
     def one_step(step, _):
         attend(step)
@@ -495,36 +517,21 @@
             down_pair("bz1u", z, 0, above, zd)
             down_pair("bz1d", z, 2, below, zu)
 
+        @pl.when(step == 4)
+        def _():
+            finish_out(1)
+            for d in range(8):
+                send_out("p", 1, d)
+                pair_sent.append(sent.pop())
+
         return 0
 
-    lax.fori_loop(0, 5, one_step, 0)
-
-    keep0 = head_lanes(0)
-    for qi in (1, 0):
-        l0 = jnp.sum(lst[qi, 0], axis=1, keepdims=True)
-        l1 = jnp.sum(lst[qi, 1], axis=1, keepdims=True)
-        outv[qi] = (acc[qi] / jnp.where(keep0, l0, l1)).astype(BF16)
-
-    def own_rows(t):
-        return pl.ds(pl.multiple_of(t * OWN, 32), OWN)
-
-    slot = tp * 2 + role
-
-    def send_out(d):
-        t, s = (tp + d) % 8, (tp + 8 - d) % 8
-        dst = (t // 2, t % 2)
-        send(
-            "p%d" % d,
-            lambda: (outv.at[1, own_rows(t)], arrived.at[slot], (pair_sp, *dst), arrived.at[s * 2 + 1 - role]),
-        )
-        if d:
-            send(
-                "a%d" % d,
-                lambda: (outv.at[0, own_rows(t)], arrived.at[slot], (sp, *dst), arrived.at[s * 2 + role]),
-            )
-
-    for d in range(8):
-        send_out(d)
+    lax.fori_loop(0, 6, one_step, 0)
+    finish_out(0)
+    for d in range(1, 8):
+        send_out("a", 0, d)
+    for wait in pair_sent:
+        wait()
     far_waits = [incoming.pop("wx1rf"), incoming.pop("wx1lf")]
     is_large = lambda: role == 1
 

time: 147 us -> 144 us (0.980)
  Pallas kernels: 145 us -> 142 us
    pallas_call x1, Pallas kernels: 145 us -> 142 us  [whole_layer(): pl.pallas_call(layer_kernel, out_shape=jax.ShapeDtypeStruct((OWN, 2048),...]
where the time goes in v7:
time: 144 us
  Pallas kernels  142 us (99%)
  local copies, waits for them, and re-layouts  1.77 us (1%)
    pallas_call x1, Pallas kernels, whole_layer(): pl.pallas_call(layer_kernel, out_shape=jax.ShapeDtypeStruct((OWN, 2048),...  142 us

profile of v7, /device:TPU:1, one launch (start us, length us, event | category | flops | bytes accessed | tf_op | source)
XLA Modules:
  0.0 144.1 jit_solution(17768418210242898587)
XLA Ops:
  0.0 142.4 %shard_map.172 = bf16[96,2048]{1,0:T(8,128)(2,1)} custom-call(bf16[768,128]{1,0:T(8,128)(2,1)} %qs_ref.1, bf16[768,128]{1,0:T(8,128)(2,1)} %ks_ref.1, bf16[768,128]{1,0:T(8,128)(2,1)} %vs_ref.1, bf16[768,128]{1,0:T(8,128)(2,1)} %ql_ref.1, bf16[768,128]{1,0:T(8,128)(2,1)} %kl_ref.1, bf16[768,128]{1,0:T(8,128)(2,1)} %vl_ref.1, f32[2,768]{1,0:T(2,128)} %bitcast.10, ...), custom_call_target="tpu_custom_call" | custom-call | flops 20000000000 | bytes 40000000 | tf_op jit(solution)/shard_map/pallas_call | solution.py:767
  142.4 1.8 %copy.20 = bf16[96,2048]{1,0:T(8,128)(2,1)} copy(bf16[96,2048]{1,0:T(8,128)(2,1)} %shard_map.172) | data formatting | bytes 786432

commit v8 on v7

--- a/solution.py
+++ b/solution.py
@@ -369,7 +369,7 @@
             jnp.where(step == 0, sp, jnp.where(step == 3, zf * 4 + x, none)),
         )
         for j in slots:
-            pl.when(j <= jnp.maximum(sp, pair_sp))(functools.partial(gate_rows, j))
+            pl.when((j <= jnp.maximum(sp, pair_sp)) & (step < 5))(functools.partial(gate_rows, j))
 
         found, count = [], 0
         for qi in range(2):
@@ -532,31 +532,14 @@
         send_out("a", 0, d)
     for wait in pair_sent:
         wait()
-    far_waits = [incoming.pop("wx1rf"), incoming.pop("wx1lf")]
-    is_large = lambda: role == 1
-
-    @pl.when(role == 1)
-    def _():
-        for wait in far_waits:
-            wait()
-
-    far_sends = [
-        pass_x2("f", zf, "wx2r", xl, right, 0, uhalf, is_large),
-        pass_x2("f", zf, "wx2l", xr, left, uhalf, uhalf, is_large),
-    ]
+    take("wx1rf", "wx1lf")
+    both_ways("f", zf)
     arrived[slot] = outv[0, own_rows(tp), :]
     take("s0", "s1", "s2", "s3")
     for d in range(8):
         take("p%d" % d)
         if d:
             take("a%d" % d)
-
-    @pl.when(role == 0)
-    def _():
-        for wait in far_waits:
-            wait()
-        for start in far_sends:
-            start()
 
     take("bz1u", "bz1d")
     down_pair("bz2u", zd, 0, above, zf)

time: 144 us -> 145 us (level)
  no operation moved by 1% of the time
where the time goes in v8:
time: 145 us; the launch traced here: 144 us
  Pallas kernels  143 us (99%)
  local copies, waits for them, and re-layouts  1.77 us (1%)
    pallas_call x1, Pallas kernels, whole_layer(): pl.pallas_call(layer_kernel, out_shape=jax.ShapeDtypeStruct((OWN, 2048),...  143 us

profile of v8, /device:TPU:1, one launch (start us, length us, event | category | flops | bytes accessed | tf_op | source)
XLA Modules:
  0.0 144.3 jit_solution(5503322128943570078)
XLA Ops:
  0.0 142.6 %shard_map.172 = bf16[96,2048]{1,0:T(8,128)(2,1)} custom-call(bf16[768,128]{1,0:T(8,128)(2,1)} %qs_ref.1, bf16[768,128]{1,0:T(8,128)(2,1)} %ks_ref.1, bf16[768,128]{1,0:T(8,128)(2,1)} %vs_ref.1, bf16[768,128]{1,0:T(8,128)(2,1)} %ql_ref.1, bf16[768,128]{1,0:T(8,128)(2,1)} %kl_ref.1, bf16[768,128]{1,0:T(8,128)(2,1)} %vl_ref.1, f32[2,768]{1,0:T(2,128)} %bitcast.10, ...), custom_call_target="tpu_custom_call" | custom-call | flops 20000000000 | bytes 40000000 | tf_op jit(solution)/shard_map/pallas_call | solution.py:750
  142.6 1.8 %copy.20 = bf16[96,2048]{1,0:T(8,128)(2,1)} copy(bf16[96,2048]{1,0:T(8,128)(2,1)} %shard_map.172) | data formatting | bytes 786432
